TPU v7x, 32 devices: a whole 2x2x4 slice. The times are simulated.
32 devices in a mesh: sp: 4 (over z), fs: 4 (over y, x), tp: 2 (over core).
Axes of the slice: x: 2, y: 2, z: 4, core: 2. Of those that a mesh axis runs over, the one named last changes fastest.
Arguments:
- tokens: bfloat16 [4, 640, 2048], P('fs', 'sp', 'tp'), may hold values from -6 to 6
- mix_gain: float32 [2048], replicated, may hold values from 0.1 to 1.9
- conv_b_weight: bfloat16 [2048, 1024], P(('sp', 'fs'), 'tp'), may hold values from -0.125 to 0.125
- conv_c_weight: bfloat16 [2048, 1024], P(('sp', 'fs'), 'tp'), may hold values from -0.125 to 0.125
- conv_v_weight: bfloat16 [2048, 1024], P(('sp', 'fs'), 'tp'), may hold values from -0.125 to 0.125
- conv_taps: float32 [3, 1024], P(None, 'tp'), may hold values from -3.5 to 3.5
- query_weight: bfloat16 [2048, 2048], P(('sp', 'fs'), 'tp'), may hold values from -0.125 to 0.125
- query_rope_weight: bfloat16 [2048, 1024], P(('sp', 'fs'), 'tp'), may hold values from -4.5 to 4.5
- latent_weight: bfloat16 [2048, 512], P(('sp', 'fs')), may hold values from -0.125 to 0.125
- key_rope_weight: bfloat16 [2048, 64], replicated, may hold values from -1 to 1
- latent_gain: float32 [512], replicated, may hold values from 0.1 to 1.9
- key_up_weight: bfloat16 [512, 2048], P(None, 'tp'), may hold values from -0.25 to 0.25
- value_up_weight: bfloat16 [512, 2048], P(None, 'tp'), may hold values from -0.25 to 0.25
- head_gain: float32 [2048], P('tp'), may hold values from 0.1 to 1.9
- conv_out_weight: bfloat16 [1024, 2048], P('tp', ('sp', 'fs')), may hold values from -0.109375 to 0.109375
- attn_out_weight: bfloat16 [2048, 2048], P('tp', ('sp', 'fs')), may hold values from -0.109375 to 0.109375
Outputs:
- mixed: bfloat16 [4, 640, 2048], P('fs', ('sp', 'tp'))
All inputs are finite; a program needn't handle non-finite values.
Results may differ from a plain program's by a relative error of at most 0.025.
Values may be sent and summed in bfloat16 or wider, within the bound.
A program may use at most 128 MiB of HBM per device.

v0:
```python
import jax
import jax.numpy as jnp
from jax import lax
from jax.sharding import PartitionSpec as P

NOPE = 128
ROPE = 64
VD = 128
KVL = 512
SEG = 64


norm_epsilon = 1e-06
rope_theta = 10000.0


def passed_along(block, axis, distance):
    devices = range(lax.axis_size(axis))
    route = [(i - distance, i) for i in devices if i - distance in devices]
    return lax.ppermute(block, axis, route)


def rms_scale(values, gain):
    return (
        values * lax.rsqrt(jnp.mean(values * values, axis=-1, keepdims=True) + norm_epsilon) * gain
    )


def rope_tables(positions):
    half_width = ROPE // 2
    frequency = rope_theta ** (-jnp.arange(half_width, dtype=jnp.float32) * 2.0 / ROPE)
    angles = positions[:, None] * frequency[None, :]
    return (jnp.cos(angles), jnp.sin(angles))


def rotate(values, cosine, sine):
    half_width = ROPE // 2
    first = values[..., :half_width]
    second = values[..., half_width:]
    return jnp.concatenate(
        [first * cosine - second * sine, second * cosine + first * sine], axis=-1
    )


def shards(
    tokens,
    mix_gain,
    conv_b_weight,
    conv_c_weight,
    conv_v_weight,
    conv_taps,
    query_weight,
    query_rope_weight,
    latent_weight,
    key_rope_weight,
    latent_gain,
    key_up_weight,
    value_up_weight,
    head_gain,
    conv_out_weight,
    attn_out_weight,
):
    full_rows = lax.all_gather(tokens[0], "tp", axis=1, tiled=True)
    tok_rows = full_rows.shape[0]
    normed = rms_scale(full_rows.astype(jnp.float32), mix_gain).astype(jnp.bfloat16)
    offset = lax.axis_index("sp") * tok_rows
    token_index = offset + jnp.arange(tok_rows, dtype=jnp.int32)
    cosine, sine = rope_tables(token_index.astype(jnp.float32))
    local_heads = query_weight.shape[1] // NOPE
    count_sp = lax.axis_size("sp")
    count_fs = lax.axis_size("fs")
    count_tp = lax.axis_size("tp")
    fs_index = lax.axis_index("fs")
    row_piece = normed.shape[1] // (count_sp * count_fs)
    all_normed = lax.all_gather(normed, "fs", axis=0, tiled=True)
    picked = lax.dynamic_index_in_dim(
        all_normed.reshape(-1, count_sp, count_fs, row_piece), fs_index, 2, keepdims=False
    ).reshape(-1, count_sp * row_piece)
    gathered = (
        lax.all_gather(conv_b_weight, "sp", axis=0, tiled=True),
        lax.all_gather(conv_c_weight, "sp", axis=0, tiled=True),
        lax.all_gather(conv_v_weight, "sp", axis=0, tiled=True),
        lax.all_gather(query_weight, "sp", axis=0, tiled=True),
        lax.all_gather(query_rope_weight, "sp", axis=0, tiled=True),
        lax.all_gather(latent_weight, "sp", axis=0, tiled=True),
    )

    def project_in():
        return jnp.concatenate(
            [jnp.dot(picked, member, preferred_element_type=jnp.float32) for member in gathered],
            axis=1,
        )

    joined = lax.psum_scatter(
        project_in().astype(jnp.bfloat16), "fs", scatter_dimension=0, tiled=True
    ).astype(jnp.float32)
    bounds = []
    running_total = 0
    for member in gathered[:-1]:
        running_total = running_total + member.shape[1]
        bounds.append(running_total)
    sums = tuple(jnp.split(joined, bounds, axis=1))
    latent_raw = sums[5].astype(jnp.bfloat16)
    gate_b = sums[0].astype(jnp.bfloat16)
    gate_c = sums[1].astype(jnp.bfloat16)
    values_v = sums[2].astype(jnp.bfloat16)
    query_nope = sums[3].astype(jnp.bfloat16).reshape(tok_rows, local_heads, NOPE)
    query_rot = rotate(
        sums[4].reshape(tok_rows, local_heads, ROPE), cosine[:, None, :], sine[:, None, :]
    ).astype(jnp.bfloat16)
    latent = rms_scale(latent_raw.astype(jnp.float32), latent_gain).astype(jnp.bfloat16)
    key_rot = rotate(
        jnp.dot(normed, key_rope_weight, preferred_element_type=jnp.float32), cosine, sine
    ).astype(jnp.bfloat16)
    query_latent = jnp.einsum(
        "thn,khn->thk",
        query_nope,
        key_up_weight.reshape(KVL, local_heads, NOPE),
        preferred_element_type=jnp.float32,
    ).astype(jnp.bfloat16)
    attn_scale = (NOPE + ROPE) ** (-0.5)
    product = (gate_c.astype(jnp.float32) * values_v.astype(jnp.float32)).astype(jnp.bfloat16)
    previous = passed_along(product[tok_rows - 2 :], "sp", 1)
    padded = jnp.concatenate([previous, product], axis=0).astype(jnp.float32)
    convolved = (
        conv_taps[0] * padded[0:tok_rows]
        + conv_taps[1] * padded[1 : tok_rows + 1]
        + conv_taps[2] * padded[2 : tok_rows + 2]
    )
    conv_y = (gate_b.astype(jnp.float32) * convolved).astype(jnp.bfloat16)
    query_segment = token_index // SEG
    last_segment = (offset + tok_rows - 1) // SEG

    def key_block(running, latent_block, rot_block, first_key):
        peak_old, denom_old, accum_old = running
        block_rows = latent_block.shape[0]
        scores = (
            jnp.einsum(
                "thk,jk->thj", query_latent, latent_block, preferred_element_type=jnp.float32
            )
            + jnp.einsum("thr,jr->thj", query_rot, rot_block, preferred_element_type=jnp.float32)
        ) * attn_scale
        key_segment = (first_key + jnp.arange(block_rows, dtype=jnp.int32)) // SEG
        allowed = key_segment[None, None, :] <= query_segment[:, None, None]
        peak_new = jnp.maximum(peak_old, jnp.max(jnp.where(allowed, scores, -1e30), axis=-1))
        weights = jnp.where(allowed, jnp.exp(scores - peak_new[..., None]), 0.0)
        rescale = jnp.exp(peak_old - peak_new)
        denom_new = denom_old * rescale + jnp.sum(weights, axis=-1)
        accum_new = accum_old * rescale[..., None] + jnp.einsum(
            "thj,jk->thk",
            weights.astype(jnp.bfloat16),
            latent_block,
            preferred_element_type=jnp.float32,
        )
        return (peak_new, denom_new, accum_new)

    starting = (
        jnp.full((tok_rows, local_heads), -1e30, jnp.float32),
        jnp.zeros((tok_rows, local_heads), jnp.float32),
        jnp.zeros((tok_rows, local_heads, KVL), jnp.float32),
    )
    latent_piece = lax.all_gather(latent, "sp", axis=0, tiled=True)
    rot_piece = lax.all_gather(key_rot, "sp", axis=0, tiled=True)
    piece_rows = latent_piece.shape[0]
    splits = max(1, piece_rows // 512)
    while piece_rows % splits:
        splits = splits - 1
    block_rows = piece_rows // splits

    def visit(state, block_index):
        block_begin = block_index * block_rows
        latent_block = lax.dynamic_slice_in_dim(latent_piece, block_begin, block_rows, 0)
        rot_block = lax.dynamic_slice_in_dim(rot_piece, block_begin, block_rows, 0)
        updated = lax.cond(
            block_begin // SEG <= last_segment,
            lambda inner: key_block(inner, latent_block, rot_block, block_begin),
            lambda inner: inner,
            state,
        )
        return (updated, None)

    peak, denom, accum = lax.scan(visit, starting, jnp.arange(splits, dtype=jnp.int32))[0]
    attended = (accum / denom[..., None]).astype(jnp.bfloat16)
    head_out = jnp.einsum(
        "thk,khv->thv",
        attended,
        value_up_weight.reshape(KVL, local_heads, VD),
        preferred_element_type=jnp.float32,
    )
    normed_heads = rms_scale(head_out, head_gain.reshape(local_heads, VD))
    attn_y = normed_heads.astype(jnp.bfloat16).reshape(tok_rows, local_heads * VD)
    share_rows = tok_rows // count_tp
    conv_all, attn_all = (
        lax.all_gather(conv_y, "fs", axis=0, tiled=True),
        lax.all_gather(attn_y, "fs", axis=0, tiled=True),
    )
    conv_sorted = (
        conv_all.reshape(count_fs, count_tp, share_rows, -1)
        .transpose(1, 0, 2, 3)
        .reshape(count_fs * tok_rows, -1)
    )
    attn_sorted = (
        attn_all.reshape(count_fs, count_tp, share_rows, -1)
        .transpose(1, 0, 2, 3)
        .reshape(count_fs * tok_rows, -1)
    )
    conv_cols_sp, attn_cols_sp = (
        lax.all_gather(conv_out_weight, "sp", axis=1, tiled=True),
        lax.all_gather(attn_out_weight, "sp", axis=1, tiled=True),
    )
    col_sums = lax.psum_scatter(
        (
            jnp.dot(conv_sorted, conv_cols_sp, preferred_element_type=jnp.float32)
            + jnp.dot(attn_sorted, attn_cols_sp, preferred_element_type=jnp.float32)
        ).astype(jnp.bfloat16),
        "tp",
        scatter_dimension=0,
        tiled=True,
    )
    col_piece = conv_cols_sp.shape[1] // count_sp
    outgoing = col_sums.reshape(count_fs, share_rows, count_sp * col_piece)
    arrived = lax.all_to_all(outgoing, "fs", split_axis=0, concat_axis=2, tiled=True)
    result = (
        arrived.reshape(share_rows, count_fs, count_sp, col_piece)
        .transpose(0, 2, 1, 3)
        .reshape(share_rows, count_fs * count_sp * col_piece)
    )
    return result[None]


def solution(mesh):
    return jax.shard_map(
        shards,
        mesh=mesh,
        in_specs=(
            P("fs", "sp", "tp"),
            P(),
            P(("sp", "fs"), "tp"),
            P(("sp", "fs"), "tp"),
            P(("sp", "fs"), "tp"),
            P(None, "tp"),
            P(("sp", "fs"), "tp"),
            P(("sp", "fs"), "tp"),
            P(("sp", "fs"), None),
            P(),
            P(),
            P(None, "tp"),
            P(None, "tp"),
            P("tp"),
            P("tp", ("sp", "fs")),
            P("tp", ("sp", "fs")),
        ),
        out_specs=P("fs", ("sp", "tp"), None),
        check_vma=False,
    )
```

profile of v0, /device:TPU:0, one launch (start us, length us, event | category | flops | bytes accessed | tf_op | source)
XLA Modules:
  0.0 311.9 jit_solution(16413146177102707444)
XLA Ops:
  6.6 2.7 all-gather
  12.2 17.5 %all_gather.44 = bf16[512,512]{1,0:T(8,128)(2,1)S(1)} all-gather(bf16[128,512]{1,0:T(8,128)(2,1)S(1)} %copy-done.9), channel_id=1, replica_groups=mesh['sp'=4,'fs'=4,'tp'=2] {'sp'}, dimensions={0}, use_global_device_ids=true | all-gather | bytes 655360 | tf_op jit(solution)/shard_map/all_gather | solution.py:80
  29.6 16.5 %all_gather.45 = bf16[512,512]{1,0:T(8,128)(2,1)} all-gather(bf16[128,512]{1,0:T(8,128)(2,1)S(1)} %copy-done.10), channel_id=1, replica_groups=mesh['sp'=4,'fs'=4,'tp'=2] {'sp'}, dimensions={0}, use_global_device_ids=true | all-gather | bytes 655360 | tf_op jit(solution)/shard_map/all_gather | solution.py:81
  46.1 16.7 %all_gather.46 = bf16[512,512]{1,0:T(8,128)(2,1)} all-gather(bf16[128,512]{1,0:T(8,128)(2,1)S(1)} %copy-done.11), channel_id=1, replica_groups=mesh['sp'=4,'fs'=4,'tp'=2] {'sp'}, dimensions={0}, use_global_device_ids=true | all-gather | bytes 655360 | tf_op jit(solution)/shard_map/all_gather | solution.py:82
  62.8 22.8 %all_gather.48 = bf16[512,512]{1,0:T(8,128)(2,1)S(1)} all-gather(bf16[128,512]{1,0:T(8,128)(2,1)S(1)} %copy-done.12), channel_id=1, replica_groups=mesh['sp'=4,'fs'=4,'tp'=2] {'sp'}, dimensions={0}, use_global_device_ids=true | all-gather | bytes 655360 | tf_op jit(solution)/shard_map/all_gather | solution.py:84
  85.6 17.8 %all_gather.49 = bf16[512,512]{1,0:T(8,128)(2,1)} all-gather(bf16[128,512]{1,0:T(8,128)(2,1)S(1)} %copy-done.13), channel_id=1, replica_groups=mesh['sp'=4,'fs'=4,'tp'=2] {'sp'}, dimensions={0}, use_global_device_ids=true | all-gather | bytes 655360 | tf_op jit(solution)/shard_map/all_gather | solution.py:85
  103.4 4.4 %copy.65 = bf16[640,2048]{0,1:T(8,128)(2,1)} copy(bf16[640,2048]{1,0:T(8,128)(2,1)} %all-gather.7.cloned.1.call-done) | data formatting | bytes 5242880 | tf_op jit(solution)/shard_map/all_gather | solution.py:75
  109.9 2.5 convolution_convert_fusion.5
  113.8 2.5 convolution_convert_fusion.4
  120.4 3.3 %fusion.15 = bf16[640,3584]{1,0:T(8,128)(2,1)} fusion(bf16[640,3584]{1,0:T(8,128)(2,1)} %constant_dynamic-update-slice_fusion, bf16[640,512]{0,1:T(8,128)(2,1)S(1)} %bitcast.104, bf16[512,1024]{1,0:T(8,128)(2,1)} %all-gather.9.cloned.1.call-done), kind=kOutput, calls=%fused_computation.35 | convolution fusion | flops 671744000 | bytes 3014656 | tf_op jit(solution)/shard_map/dot_general | solution.py:90
  130.3 14.1 %all-gather.1 = bf16[4,160,64]{1,2,0:T(8,128)(2,1)} all-gather(bf16[1,160,64]{1,2,0:T(8,128)(2,1)S(1)} %maximum_bitcast_fusion), channel_id=1, replica_groups=mesh['sp'=4,'fs'=4,'tp'=2] {'sp'}, dimensions={0}, use_global_device_ids=true | all-gather | bytes 102400 | tf_op jit(solution)/shard_map/all_gather | solution.py:163
  144.3 36.4 %reduce-scatter.3.cloned.1.call-done = bf16[160,3584]{1,0:T(8,128)(2,1)} async-done(((bf16[640,3584]{1,0:T(8,128)(2,1)}), bf16[160,3584]{1,0:T(8,128)(2,1)}) %reduce-scatter.3.cloned.1.call-update) | async-done | bytes 1146896 | tf_op jit(solution)/shard_map/reduce_scatter | solution.py:94
  183.6 17.8 %all_gather.52 = bf16[640,512]{1,0:T(8,128)(2,1)S(1)} all-gather(bf16[160,512]{1,0:T(8,128)(2,1)S(1)} %get-tuple-element.251), channel_id=1, replica_groups=mesh['sp'=4,'fs'=4,'tp'=2] {'sp'}, dimensions={0}, use_global_device_ids=true | all-gather | bytes 819200 | tf_op jit(solution)/shard_map/all_gather | solution.py:162
  204.5 12.2 %conditional.1 = ((f32[160,8]{1,0:T(8,128)S(1)}, f32[160,8,512]{2,1,0:T(8,128)})) conditional(s32[]{:T(128)} %convert_element_type.79, (f32[160,8]{1,0:T(8,128)S(1)}, f32[160,8,512]{2,1,0:T(8,128)}) %tuple.31, (s32[160]{0:T(256)S(1)}, s32[160]{0:T(256)S(1)}, s32[]{:T(128)}, bf16[160,8,512]{2,0,1:T(8,128)(2,1)S(1)}, ...), branch_computations={%region_3.4_spmd, %region_4.7_spmd.clone} | conditional | flops 1792195712 | bytes 46272084 | solution.py:174
  209.7 1.9 select_reduce_fusion
  216.7 2.1 divide_convert_fusion
  221.6 2.5 collective-permute-start
  224.1 15.4 %all_gather.51 = bf16[512,512]{1,0:T(8,128)(2,1)S(1)} all-gather(bf16[512,128]{1,0:T(8,128)(2,1)S(1)} %copy-done.14), channel_id=1, replica_groups=mesh['sp'=4,'fs'=4,'tp'=2] {'sp'}, dimensions={1}, use_global_device_ids=true | all-gather | bytes 655360 | tf_op jit(solution)/shard_map/all_gather | solution.py:208
  240.6 12.5 %all_gather.50 = bf16[640,512]{1,0:T(8,128)(2,1)S(1)} all-gather(bf16[160,512]{1,0:T(8,128)(2,1)S(1)} %fusion.40), channel_id=1, replica_groups=mesh['sp'=4,'fs'=4,'tp'=2] {'fs'}, dimensions={0}, use_global_device_ids=true | all-gather | bytes 819200 | tf_op jit(solution)/shard_map/all_gather | solution.py:194
  253.6 2.5 copy.81
  256.1 26.6 %all-gather.13.cloned.1.call-done = bf16[1024,512]{1,0:T(8,128)(2,1)} async-done(((bf16[1024,128]{1,0:T(8,128)(2,1)}), bf16[1024,512]{1,0:T(8,128)(2,1)}) %all-gather.13.cloned.1.call-update) | async-done | bytes 1048592 | tf_op jit(solution)/shard_map/all_gather | solution.py:209
  282.8 3.3 %fusion.17 = bf16[640,512]{1,0:T(8,128)(2,1)} fusion(f32[640,512]{1,0:T(8,128)S(1)} %fusion.44, bf16[640,1024]{1,0:T(8,128)(2,1)} %bitcast.98, bf16[1024,512]{1,0:T(8,128)(2,1)} %all-gather.13.cloned.1.call-done), kind=kOutput, calls=%fused_computation.38 | convolution fusion | flops 671744000 | bytes 4325376 | tf_op jit(solution)/shard_map/dot_general | solution.py:214
  286.1 6.5 %reduce-scatter.5.cloned.1.call-done = bf16[320,512]{1,0:T(8,128)(2,1)} async-done(((bf16[640,512]{1,0:T(8,128)(2,1)}), bf16[320,512]{1,0:T(8,128)(2,1)}) %reduce-scatter.5.cloned.1.call-update) | async-done | bytes 327696 | tf_op jit(solution)/shard_map/reduce_scatter | solution.py:211
  292.6 11.0 %all_to_all.15 = bf16[4,80,512]{2,1,0:T(8,128)(2,1)S(1)} all-to-all(bf16[4,80,512]{2,1,0:T(8,128)(2,1)} %bitcast.107), channel_id=1, replica_groups=mesh['sp'=4,'fs'=4,'tp'=2] {'fs'}, dimensions={0} | all-to-all | bytes 655360 | tf_op jit(solution)/shard_map/all_to_all | solution.py:222
  (107 shorter events, 38.7 us)
Async XLA Ops:
  6.5 196.5 %copy-start = (bf16[512,1024]{1,0:T(8,128)(2,1)S(1)}, bf16[512,1024]{1,0:T(8,128)(2,1)}, u32[]{:S(2)}) copy-start(bf16[512,1024]{1,0:T(8,128)(2,1)} %param.29) | copy-start | bytes 3145732
  6.5 5.6 %copy-start.9 = (bf16[128,512]{1,0:T(8,128)(2,1)S(1)}, bf16[128,512]{1,0:T(8,128)(2,1)}, u32[]{:S(2)}) copy-start(bf16[128,512]{1,0:T(8,128)(2,1)} %param.20) | copy-start | bytes 393220
  6.5 23.1 %copy-start.10 = (bf16[128,512]{1,0:T(8,128)(2,1)S(1)}, bf16[128,512]{1,0:T(8,128)(2,1)}, u32[]{:S(2)}) copy-start(bf16[128,512]{1,0:T(8,128)(2,1)} %param.21) | copy-start | bytes 393220
  6.5 39.6 %copy-start.11 = (bf16[128,512]{1,0:T(8,128)(2,1)S(1)}, bf16[128,512]{1,0:T(8,128)(2,1)}, u32[]{:S(2)}) copy-start(bf16[128,512]{1,0:T(8,128)(2,1)} %param.22) | copy-start | bytes 393220
  6.5 96.9 %all-gather.7.cloned.1.call-start = ((), (), s32[]{:S(2)}) async-start(), calls=%async_computation.3 | async-start | bytes 3276800 | tf_op jit(solution)/shard_map/all_gather | solution.py:75
  9.3 53.5 %copy-start.12 = (bf16[128,512]{1,0:T(8,128)(2,1)S(1)}, bf16[128,512]{1,0:T(8,128)(2,1)}, u32[]{:S(2)}) copy-start(bf16[128,512]{1,0:T(8,128)(2,1)} %param.25) | copy-start | bytes 393220
  9.3 76.3 %copy-start.13 = (bf16[128,512]{1,0:T(8,128)(2,1)S(1)}, bf16[128,512]{1,0:T(8,128)(2,1)}, u32[]{:S(2)}) copy-start(bf16[128,512]{1,0:T(8,128)(2,1)} %param.26) | copy-start | bytes 393220
  11.4 109.0 %all-gather.9.cloned.1.call-start = ((), (), s32[]{:S(2)}) async-start(), calls=%async_computation.4 | async-start | bytes 1310720 | tf_op jit(solution)/shard_map/all_gather | solution.py:83
  12.1 168.6 %reduce-scatter.3.cloned.1.call-start = ((), (), s32[]{:S(2)}) async-start(), calls=%async_computation.5 | async-start | bytes 5734400 | tf_op jit(solution)/shard_map/reduce_scatter | solution.py:94
  109.0 4.8 %copy-start.5 = (bf16[640,4,1,128]{0,3,2,1:T(8,128)(2,1)}, bf16[640,4,1,128]{0,3,2,1:T(8,128)(2,1)S(1)}, u32[]{:S(2)}) copy-start(bf16[640,4,1,128]{0,3,2,1:T(8,128)(2,1)S(1)} %constant_dynamic-slice_fusion) | copy-start | bytes 1966084
  118.5 1.8 copy-start.6
  120.4 4.7 %copy-start.7 = (bf16[512,512]{1,0:T(8,128)(2,1)S(1)}, bf16[512,512]{1,0:T(8,128)(2,1)}, u32[]{:S(2)}) copy-start(bf16[512,512]{1,0:T(8,128)(2,1)} %all_gather.49) | copy-start | bytes 1572868
  126.5 1.1 copy-start.8
  126.5 55.3 %copy-start.17 = (f32[512]{0:T(512)S(1)}, f32[512]{0:T(512)}, u32[]{:S(2)}) copy-start(f32[512]{0:T(512)} %param.28) | copy-start | bytes 6148
  126.5 127.1 %all-gather.11.cloned.1.call-start = ((), (), s32[]{:S(2)}) async-start(), calls=%async_computation.6 | async-start | bytes 1638400 | tf_op jit(solution)/shard_map/all_gather | solution.py:195
  211.6 1.7 copy-start.1
  215.1 1.5 copy-start.2
  216.7 2.1 copy-start.18
  218.8 2.8 copy-start.15
  218.8 2.8 copy-start.4
  218.8 5.3 %copy-start.14 = (bf16[512,128]{1,0:T(8,128)(2,1)S(1)}, bf16[512,128]{1,0:T(8,128)(2,1)}, u32[]{:S(2)}) copy-start(bf16[512,128]{1,0:T(8,128)(2,1)} %param.32) | copy-start | bytes 393220
  220.9 61.9 %all-gather.13.cloned.1.call-start = ((), (), s32[]{:S(2)}) async-start(), calls=%async_computation.7 | async-start | bytes 1310720 | tf_op jit(solution)/shard_map/all_gather | solution.py:209
  221.5 71.1 %reduce-scatter.5.cloned.1.call-start = ((), (), s32[]{:S(2)}) async-start(), calls=%async_computation.8 | async-start | bytes 983040 | tf_op jit(solution)/shard_map/reduce_scatter | solution.py:211
  221.6 17.9 %collective-permute-start = (bf16[2,512]{1,0:T(2,128)(2,1)S(1)}, bf16[2,512]{1,0:T(2,128)(2,1)S(1)}, u32[]{:S(2)}, u32[]{:S(2)}) collective-permute-start(bf16[2,512]{1,0:T(2,128)(2,1)S(1)} %slice.44), channel_id=1, source_target_pairs={{0,8},{8,16},{16,24},{1,9},{9,17},{17,25},{2,10},{10,18},{18,26},{... | collective-permute-start | bytes 6152 | tf_op jit(solution)/shard_map/ppermute | solution.py:20
  (2 other events, 2.2 us)
Sparse Core Ops, SparseCore 0:
  11.5 42.1 all-gather.6
  55.2 39.4 all-gather.8
  126.6 54.0 reduce-scatter.2
  221.0 30.3 all-gather.10
  252.8 29.8 all-gather.12
  286.2 6.3 reduce-scatter.4
where the time goes:
time: 313 us; the launch traced here: 312 us
  blocking collectives  165 us (53%)
  waiting for transfers between devices  70.9 us (23%)
  local copies, waits for them, and re-layouts  23.9 us (8%)
  matrix products  23.6 us (8%)
  between operations  13.8 us (4%)
  other arithmetic  12 us (4%)
    reduce_scatter x1, waiting for transfers between devices, shards(): lax.psum_scatter(project_in().astype(jnp.bfloat16), 'fs', scatter_dimensi...  36.4 us
    all_gather x1, waiting for transfers between devices, shards(): lax.all_gather(attn_out_weight, 'sp', axis=1, tiled=True)  26.6 us
    all_gather x1, blocking collectives, shards(): lax.all_gather(query_rope_weight, 'sp', axis=0, tiled=True)  22.8 us
    all_gather x1, blocking collectives, shards(): lax.all_gather(latent_weight, 'sp', axis=0, tiled=True)  17.8 us
    all_gather x1, blocking collectives, shards(): latent_piece = lax.all_gather(latent, 'sp', axis=0, tiled=True)  17.8 us
    all_gather x1, blocking collectives, shards(): lax.all_gather(conv_b_weight, 'sp', axis=0, tiled=True)  17.5 us
    all_gather x1, blocking collectives, shards(): lax.all_gather(conv_v_weight, 'sp', axis=0, tiled=True)  16.7 us
    all_gather x1, blocking collectives, shards(): lax.all_gather(conv_c_weight, 'sp', axis=0, tiled=True)  16.5 us
  transfers between devices with their start and end apart: 7, of which 3 were waited for; matrix products, arithmetic and copies ran while one was open for 8% of the time, Pallas kernels for 0%

commit v1 on v0

--- a/solution.py
+++ b/solution.py
@@ -1,6 +1,10 @@
+import functools
+
 import jax
 import jax.numpy as jnp
 from jax import lax
+from jax.experimental import pallas as pl
+from jax.experimental.pallas import tpu as pltpu
 from jax.sharding import PartitionSpec as P
 
 NOPE = 128
@@ -42,7 +46,7 @@
     )
 
 
-def shards(
+def general_shards(
     tokens,
     mix_gain,
     conv_b_weight,
@@ -228,9 +232,560 @@
     return result[None]
 
 
+MESH = pl.DeviceIdType.MESH
+
+
+class Place:
+    def __init__(self):
+        self.z = lax.axis_index("sp")
+        self.f = lax.axis_index("fs")
+        self.c = lax.axis_index("tp")
+
+    def to(self, z=None, f=None, c=None):
+        return {
+            "sp": self.z if z is None else z,
+            "fs": self.f if f is None else f,
+            "tp": self.c if c is None else c,
+        }
+
+
+def flip(index, bit):
+    digit = (index // bit) % 2
+    return index + bit * (1 - 2 * digit)
+
+
+def remote(src, dst, send, recv, device):
+    return pltpu.make_async_remote_copy(
+        src_ref=src, dst_ref=dst, send_sem=send, recv_sem=recv, device_id=device, device_id_type=MESH
+    )
+
+
+def greet(devices):
+    barrier = pltpu.get_barrier_semaphore()
+    for device in devices:
+        pl.semaphore_signal(barrier, inc=1, device_id=device, device_id_type=MESH)
+    pl.semaphore_wait(barrier, len(devices))
+
+
+def gather_kernel(
+    n,
+    tok_in,
+    gain,
+    cb,
+    cc,
+    cv,
+    qw,
+    qr,
+    lw,
+    krw,
+    co,
+    ao,
+    proj_out,
+    lat_out,
+    krot_out,
+    wout,
+    tok,
+    normed,
+    win,
+    lat,
+    wsem,
+    lsem,
+    tsem,
+    psem,
+    latsem,
+):
+    here = Place()
+    z, f, c = here.z, here.f, here.c
+    fx, fy = flip(f, 1), flip(f, 2)
+    other = 1 - c
+    rows = cb.shape[0]
+    members = (cb, cc, cv, qw, qr, lw)
+    widths = [m.shape[1] // n for m in members]
+    starts = [sum(widths[:i]) for i in range(len(widths))]
+    total = sum(widths)
+    lat_w = widths[-1]
+    proj_w = total - lat_w
+    tr = tok_in.shape[1]
+    length = n * tr
+    half = length // 2
+    outs = (co, ao)
+    heights = [m.shape[0] // n for m in outs]
+    tops = [sum(heights[:i]) for i in range(len(heights))]
+    out_cols = co.shape[1]
+
+    steps = [(1 + j, s) for j in range(n - 1) for s in (-1, 1)]
+
+    greet(
+        [here.to(z=lax.rem(z + j, n)) for j in range(1, n)]
+        + [here.to(f=fx), here.to(f=fy), here.to(c=other)]
+    )
+
+    def in_block(zs, fs):
+        return win.at[pl.ds(pl.multiple_of((zs * 4 + fs) * rows, rows), rows), :]
+
+    def out_block(zs, fs):
+        return wout.at[:, pl.ds(pl.multiple_of((zs * 4 + fs) * out_cols, out_cols), out_cols)]
+
+    blocks = (in_block, out_block)
+
+    def pieces(kind, dest):
+        found = []
+        if kind == 0:
+            dst = (z * 4 + f) * rows
+            for m, w, s in zip(members, widths, starts):
+                src = m.at[:, pl.ds(pl.multiple_of(dest * w, w), w)]
+                found.append((src, win.at[pl.ds(pl.multiple_of(dst, rows), rows), pl.ds(s, w)]))
+        else:
+            dst = (z * 4 + f) * out_cols
+            for m, h, s in zip(outs, heights, tops):
+                src = m.at[pl.ds(pl.multiple_of(dest * h, h), h), :]
+                found.append((src, wout.at[pl.ds(s, h), pl.ds(pl.multiple_of(dst, out_cols), out_cols)]))
+        return found
+
+    def send_own(kind):
+        for src, dst in pieces(kind, z):
+            remote(src, dst, wsem.at[kind, 2, z], wsem.at[kind, 3, z], here.to(f=fx)).start()
+            remote(src, dst, wsem.at[kind, 4, z], wsem.at[kind, 5, z], here.to(f=fy)).start()
+            pltpu.make_async_copy(src, dst, lsem.at[kind]).start()
+
+    def send_z(kind, distance, sign):
+        dest = z + sign * distance
+
+        @pl.when((dest >= 0) & (dest < n))
+        def _():
+            for src, dst in pieces(kind, dest):
+                remote(src, dst, wsem.at[kind, 0, dest], wsem.at[kind, 1, z], here.to(z=dest)).start()
+
+    def plane_copy(kind, zs, role, fs, to):
+        block = blocks[kind](zs, fs)
+        return remote(block, block, wsem.at[kind, role, zs], wsem.at[kind, role + 1, zs], here.to(f=to))
+
+    def relay_z(kind, distance, sign):
+        zs = z + sign * distance
+
+        @pl.when((zs >= 0) & (zs < n))
+        def _():
+            block = blocks[kind](zs, f)
+            remote(block, block, wsem.at[kind, 0, zs], wsem.at[kind, 1, zs], here.to(z=zs)).wait_recv()
+            plane_copy(kind, zs, 2, f, fx).start()
+            plane_copy(kind, zs, 4, f, fy).start()
+
+    def relay_plane(kind, zs):
+        plane_copy(kind, zs, 2, fx, fx).wait_recv()
+
+        @pl.when(zs % 2 == 0)
+        def _():
+            plane_copy(kind, zs, 6, fx, fy).start()
+
+        plane_copy(kind, zs, 4, fy, fy).wait_recv()
+
+        @pl.when(zs % 2 == 1)
+        def _():
+            plane_copy(kind, zs, 6, fy, fx).start()
+
+    def tok_block(half_index, zs):
+        return tok.at[half_index, pl.ds(pl.multiple_of(zs * tr, tr), tr), :]
+
+    def tok_copy(zs, sign, hop, src=None):
+        d = (sign + 1) // 2
+        block = tok_block(c, zs)
+        return remote(
+            block if src is None else src, block, tsem.at[d, 0, hop], tsem.at[d, 1, hop], here.to(z=z + sign)
+        )
+
+    def partner_copy(zs, owner, src=None):
+        block = tok_block(owner, zs)
+        return remote(block if src is None else src, block, psem.at[0, zs], psem.at[1, zs], here.to(c=other))
+
+    own_tok = tok_in.at[0]
+
+    def can(sign):
+        return (z + sign >= 0) & (z + sign < n)
+
+    send_own(0)
+    for distance, sign in steps[:2]:
+        send_z(0, distance, sign)
+    partner_copy(z, c, own_tok).start()
+    pltpu.make_async_copy(own_tok, tok_block(c, z), lsem.at[2]).start()
+    for sign in (-1, 1):
+        pl.when(can(sign))(lambda sign=sign: tok_copy(z, sign, 0, own_tok).start())
+    for distance, sign in steps[2:]:
+        send_z(0, distance, sign)
+
+    def relay_tok(distance, sign):
+        zs = z + sign * distance
+
+        @pl.when((zs >= 0) & (zs < n))
+        def _():
+            tok_copy(zs, -sign, distance - 1).wait_recv()
+            if distance < n - 1:
+                pl.when(can(-sign))(lambda: tok_copy(zs, -sign, distance).start())
+            partner_copy(zs, c).start()
+
+    for distance, sign in steps:
+        relay_z(0, distance, sign)
+        relay_tok(distance, sign)
+    send_own(1)
+    for distance, sign in steps:
+        send_z(1, distance, sign)
+
+    def each_zs(fn):
+        def body(i, carry):
+            fn(lax.rem(z + i, n))
+            return carry
+
+        lax.fori_loop(0, n, body, 0)
+
+    def tok_ready(zs):
+        partner_copy(zs, other).wait_recv()
+
+    each_zs(tok_ready)
+    pltpu.make_async_copy(own_tok, tok_block(c, z), lsem.at[2]).wait()
+    chunk = tr // 2
+    wide = tok.shape[2]
+
+    def norm_chunk(i, carry):
+        at = pl.ds(pl.multiple_of(i * chunk, chunk), chunk)
+        first = tok[0, at, :].astype(jnp.float32)
+        second = tok[1, at, :].astype(jnp.float32)
+        mean = (
+            jnp.sum(first * first, axis=-1, keepdims=True) + jnp.sum(second * second, axis=-1, keepdims=True)
+        ) / (2 * wide)
+        scale = lax.rsqrt(mean + norm_epsilon)
+        normed[at, 0:wide] = (first * scale * gain[0, :]).astype(jnp.bfloat16)
+        normed[at, wide : 2 * wide] = (second * scale * gain[1, :]).astype(jnp.bfloat16)
+        return carry
+
+    each_zs(lambda zs: relay_plane(0, zs))
+    lax.fori_loop(0, 2 * n, norm_chunk, 0)
+    for distance, sign in steps:
+        relay_z(1, distance, sign)
+
+    def relay_done(kind, zs):
+        plane_copy(kind, zs, 6, flip(fx, 2), fx).wait_recv()
+
+    for src, dst in pieces(0, z)[:1]:
+        pltpu.make_async_copy(in_block(z, f), in_block(z, f), lsem.at[0]).wait()
+    each_zs(lambda zs: relay_done(0, zs))
+
+    def lat_block(zs, owner):
+        return lat.at[zs, pl.ds(pl.multiple_of(owner * half, half), half), :]
+
+    def lat_copy(dest):
+        return remote(lat_block(z, c), lat_block(z, c), latsem.at[0, dest], latsem.at[1, z], here.to(z=dest))
+
+    def lat_arrival(zs):
+        return remote(lat_block(zs, c), lat_block(zs, c), latsem.at[0, zs], latsem.at[1, zs], here.to(z=zs))
+
+    def lat_partner(zs, owner):
+        return remote(
+            lat_block(zs, owner), lat_block(zs, owner), latsem.at[2, zs], latsem.at[3, zs], here.to(c=other)
+        )
+
+    mine = pl.ds(pl.multiple_of(c * half, half), half)
+    lat[z, mine, :] = jnp.dot(
+        normed[mine, :], win[:, proj_w:total], preferred_element_type=jnp.float32
+    ).astype(jnp.bfloat16)
+    for j in range(1, n):
+        lat_copy(lax.rem(z + j, n)).start()
+    lat_partner(z, c).start()
+    each_zs(lambda zs: relay_plane(1, zs))
+
+    def project(i, carry):
+        at = pl.ds(pl.multiple_of(i * tr, tr), tr)
+        proj_out[at, :] = jnp.dot(
+            normed[at, :], win[:, 0:proj_w], preferred_element_type=jnp.float32
+        ).astype(jnp.bfloat16)
+        krot_out[at, :] = jnp.dot(normed[at, :], krw[...], preferred_element_type=jnp.float32)
+        return carry
+
+    lax.fori_loop(0, n, project, 0)
+    for j in range(1, n):
+        zs = lax.rem(z + j, n)
+        lat_arrival(zs).wait_recv()
+        lat_partner(zs, c).start()
+    each_zs(lambda zs: lat_partner(zs, other).wait_recv())
+    for k in range(n):
+        lat_out[:, k * lat_w : (k + 1) * lat_w] = lat[k]
+
+    pltpu.make_async_copy(out_block(z, f), out_block(z, f), lsem.at[1]).wait()
+    each_zs(lambda zs: relay_done(1, zs))
+    for j in range(1, n):
+        zs = lax.rem(z + j, n)
+        for kind in (0, 1):
+            block = blocks[kind](zs, f)
+            remote(block, block, wsem.at[kind, 0, zs], wsem.at[kind, 1, zs], here.to(z=zs)).wait_send()
+        lat_copy(zs).wait_send()
+
+    def sent(zs):
+        for kind in (0, 1):
+            plane_copy(kind, zs, 2, f, fx).wait_send()
+            plane_copy(kind, zs, 4, f, fy).wait_send()
+            plane_copy(kind, zs, 6, fx, fy).wait_send()
+        partner_copy(zs, c).wait_send()
+        lat_partner(zs, c).wait_send()
+
+    each_zs(sent)
+    for sign in (-1, 1):
+        pl.when(can(sign))(lambda sign=sign: tok_copy(z, sign, 0).wait_send())
+        for distance in range(1, n - 1):
+            zs = z - sign * distance
+            pl.when((zs >= 0) & (zs < n) & can(sign))(
+                lambda sign=sign, distance=distance: tok_copy(z, sign, distance).wait_send()
+            )
+
+
+def reduce_kernel(n, part, out, own, pair, moving, fetched, csem, psem, zsem):
+    here = Place()
+    z, c = here.z, here.c
+    other = 1 - c
+    share = out.shape[0]
+    greet(
+        [here.to(c=other)]
+        + [here.to(z=lax.rem(z + 1, n)), here.to(z=lax.rem(z + n - 1, n))]
+    )
+
+    def rows(zs, core):
+        return part.at[pl.ds(pl.multiple_of((2 * zs + core) * share, share), share), :]
+
+    def pair_copy(zs):
+        return remote(rows(zs, other), pair.at[zs], psem.at[0, zs], psem.at[1, zs], here.to(c=other))
+
+    def own_copy(zs):
+        return pltpu.make_async_copy(rows(zs, c), own.at[zs], csem.at[zs])
+
+    order = [j for j in range(n - 1, -1, -1)]
+
+    def line_copy(d, dest):
+        return remote(
+            moving.at[d, dest],
+            fetched.at[d, dest],
+            zsem.at[d, 0, dest],
+            zsem.at[d, 1, dest],
+            here.to(z=z + 2 * d - 1),
+        )
+
+    turns = [(far, d) for far in range(n - 1, -1, -1) for d in (0, 1)]
+    for far, d in turns:
+        dest = z + (2 * d - 1) * far
+        if far == 0 and d == 1:
+            continue
+
+        @pl.when((dest >= 0) & (dest < n))
+        def _():
+            pair_copy(dest).start()
+            own_copy(dest).start()
+
+    def summed(dest):
+        return own[dest].astype(jnp.float32) + pair[dest].astype(jnp.float32)
+
+    for far, d in turns:
+        dest = z + (2 * d - 1) * far
+        if far == 0:
+            continue
+
+        @pl.when((dest >= 0) & (dest < n))
+        def _():
+            own_copy(dest).wait()
+            pair_copy(dest).wait_recv()
+            before = z - (2 * d - 1)
+            has = (before >= 0) & (before < n)
+
+            @pl.when(has)
+            def _():
+                line_copy(d, dest).wait_recv()
+                moving[d, dest] = (summed(dest) + fetched[d, dest].astype(jnp.float32)).astype(jnp.bfloat16)
+
+            @pl.when(jnp.logical_not(has))
+            def _():
+                moving[d, dest] = summed(dest).astype(jnp.bfloat16)
+
+            line_copy(d, dest).start()
+
+    own_copy(z).wait()
+    pair_copy(z).wait_recv()
+    low, high = z > 0, z < n - 1
+
+    @pl.when(low)
+    def _():
+        line_copy(1, z).wait_recv()
+
+    @pl.when(high)
+    def _():
+        line_copy(0, z).wait_recv()
+
+    result = summed(z)
+    from_low = fetched[1, z].astype(jnp.float32)
+    from_high = fetched[0, z].astype(jnp.float32)
+    zero = jnp.zeros_like(result)
+    result = result + jnp.where(low, from_low, zero) + jnp.where(high, from_high, zero)
+    out[...] = result.astype(jnp.bfloat16)
+
+    for far, d in turns:
+        dest = z + (2 * d - 1) * far
+        if far == 0 and d == 1:
+            continue
+
+        @pl.when((dest >= 0) & (dest < n))
+        def _():
+            pair_copy(dest).wait_send()
+            if far:
+                line_copy(d, dest).wait_send()
+
+
+def split_shards(
+    tokens,
+    mix_gain,
+    conv_b_weight,
+    conv_c_weight,
+    conv_v_weight,
+    conv_taps,
+    query_weight,
+    query_rope_weight,
+    latent_weight,
+    key_rope_weight,
+    latent_gain,
+    key_up_weight,
+    value_up_weight,
+    head_gain,
+    conv_out_weight,
+    attn_out_weight,
+):
+    n = lax.axis_size("sp")
+    z = lax.axis_index("sp")
+    tr = tokens.shape[1]
+    wide = tokens.shape[2]
+    length = n * tr
+    features = 2 * wide
+    heads = query_weight.shape[1] // NOPE // n
+    channels = conv_b_weight.shape[1] // n
+    lat_w = latent_weight.shape[1] // n
+    proj_w = 3 * channels + heads * (NOPE + ROPE)
+    out_rows = (conv_out_weight.shape[0] + attn_out_weight.shape[0]) // n
+    columns = attn_out_weight.shape[1] * n * 4
+    bf16 = jnp.bfloat16
+    vmem = pl.BlockSpec(memory_space=pltpu.VMEM)
+    anywhere = pl.BlockSpec(memory_space=pl.ANY)
+    dma = pltpu.SemaphoreType.DMA
+    proj, lat_raw, krot_raw, wout = pl.pallas_call(
+        functools.partial(gather_kernel, n),
+        out_shape=(
+            jax.ShapeDtypeStruct((length, proj_w), bf16),
+            jax.ShapeDtypeStruct((length, n * lat_w), bf16),
+            jax.ShapeDtypeStruct((length, ROPE), jnp.float32),
+            jax.ShapeDtypeStruct((out_rows, columns), bf16),
+        ),
+        in_specs=[anywhere, vmem] + [anywhere] * 6 + [vmem] + [anywhere] * 2,
+        out_specs=(vmem, vmem, vmem, anywhere),
+        scratch_shapes=[
+            pltpu.VMEM((2, length, wide), bf16),
+            pltpu.VMEM((length, features), bf16),
+            pltpu.VMEM((features, proj_w + lat_w), bf16),
+            pltpu.VMEM((n, length, lat_w), bf16),
+            dma((2, 8, n)),
+            dma((3,)),
+            dma((2, 2, n)),
+            dma((2, n)),
+            dma((4, n)),
+        ],
+        compiler_params=pltpu.CompilerParams(
+            collective_id=0, has_side_effects=True, vmem_limit_bytes=48 * 1024 * 1024
+        ),
+        name="gather_project",
+    )(
+        tokens,
+        mix_gain.reshape(2, wide),
+        conv_b_weight,
+        conv_c_weight,
+        conv_v_weight,
+        query_weight,
+        query_rope_weight,
+        latent_weight,
+        key_rope_weight,
+        conv_out_weight,
+        attn_out_weight,
+    )
+    f32 = jnp.float32
+
+    def mine(array, axis):
+        width = array.shape[axis] // n
+        return lax.dynamic_slice_in_dim(array, z * width, width, axis)
+
+    taps = mine(conv_taps, 1)
+    key_up = mine(key_up_weight, 1)
+    value_up = mine(value_up_weight, 1)
+    gain = mine(head_gain, 0).reshape(heads, VD)
+    cosine, sine = rope_tables(jnp.arange(length, dtype=f32))
+    gate_b, gate_c, values_v = (proj[:, i * channels : (i + 1) * channels].astype(f32) for i in range(3))
+    at = 3 * channels
+    query_nope = proj[:, at : at + heads * NOPE].reshape(length, heads, NOPE)
+    at = at + heads * NOPE
+    query_rot = rotate(
+        proj[:, at:].astype(f32).reshape(length, heads, ROPE), cosine[:, None, :], sine[:, None, :]
+    ).astype(bf16)
+    product = (gate_c * values_v).astype(bf16)
+    padded = jnp.concatenate([jnp.zeros((2, channels), bf16), product], axis=0).astype(f32)
+    convolved = taps[0] * padded[0:length] + taps[1] * padded[1 : length + 1] + taps[2] * padded[2 : length + 2]
+    conv_y = (gate_b * convolved).astype(bf16)
+    latent = rms_scale(lat_raw.astype(f32), latent_gain).astype(bf16)
+    key_rot = rotate(krot_raw, cosine, sine).astype(bf16)
+    keys = jnp.dot(latent, key_up, preferred_element_type=f32).astype(bf16).reshape(length, heads, NOPE)
+    values = jnp.dot(latent, value_up, preferred_element_type=f32).astype(bf16).reshape(length, heads, VD)
+    scores = (
+        jnp.einsum("thn,jhn->htj", query_nope, keys, preferred_element_type=f32)
+        + jnp.einsum("thr,jr->htj", query_rot, key_rot, preferred_element_type=f32)
+    ) * (NOPE + ROPE) ** (-0.5)
+    segment = jnp.arange(length, dtype=jnp.int32) // SEG
+    allowed = segment[None, None, :] <= segment[None, :, None]
+    scores = jnp.where(allowed, scores, -1e30)
+    weights = jnp.exp(scores - jnp.max(scores, axis=-1, keepdims=True))
+    denom = jnp.sum(weights, axis=-1)
+    head_out = jnp.einsum("htj,jhv->thv", weights.astype(bf16), values, preferred_element_type=f32)
+    head_out = head_out / denom.T[:, :, None]
+    attn_y = rms_scale(head_out, gain).astype(bf16).reshape(length, heads * VD)
+    mixed_y = jnp.concatenate([conv_y, attn_y], axis=1)
+    part = jnp.dot(mixed_y, wout, preferred_element_type=f32).astype(bf16)
+    share = tr // 2
+    result = pl.pallas_call(
+        functools.partial(reduce_kernel, n),
+        out_shape=jax.ShapeDtypeStruct((share, columns), bf16),
+        in_specs=[anywhere],
+        out_specs=vmem,
+        scratch_shapes=[
+            pltpu.VMEM((n, share, columns), bf16),
+            pltpu.VMEM((n, share, columns), bf16),
+            pltpu.VMEM((2, n, share, columns), bf16),
+            pltpu.VMEM((2, n, share, columns), bf16),
+            dma((n,)),
+            dma((2, n)),
+            dma((2, 2, n)),
+        ],
+        compiler_params=pltpu.CompilerParams(
+            collective_id=1, has_side_effects=True, vmem_limit_bytes=32 * 1024 * 1024
+        ),
+        name="reduce_partials",
+    )(part)
+    return result[None]
+
+
+def splits_well(mesh):
+    n = mesh.shape["sp"]
+    return n > 2 and n <= 4 and mesh.shape["fs"] == 4 and mesh.shape["tp"] == 2
+
+
+def shards(*arrays):
+    n = lax.axis_size("sp")
+    conv, query, rope, low_rank = (arrays[i].shape[1] for i in (2, 6, 7, 8))
+    heads = query // NOPE
+    even = heads % n == 0 and all(w % (128 * n) == 0 for w in (conv, query, rope, low_rank))
+    if even and arrays[0].shape[1] % 32 == 0 and arrays[15].shape[1] % 128 == 0:
+        return split_shards(*arrays)
+    return general_shards(*arrays)
+
+
 def solution(mesh):
     return jax.shard_map(
-        shards,
+        shards if splits_well(mesh) else general_shards,
         mesh=mesh,
         in_specs=(
             P("fs", "sp", "tp"),

time: 313 us -> 138 us (0.44)
  blocking collectives: 165 us -> 0 us
  Pallas kernels: 0 us -> 106 us
  waiting for transfers between devices: 70.9 us -> 0 us
  between operations: 13.8 us -> 0.16 us
  matrix products: 23.6 us -> 11.9 us
  local copies, waits for them, and re-layouts: 23.9 us -> 15 us
  other arithmetic: 12 us -> 3.49 us
    all_gather x10 -> x0, blocking collectives: 154 us -> none  [the longest x1 22.8 us: shards(): lax.all_gather(query_rope_weight, 'sp', axis=0, tiled=True)]
    pallas_call x0 -> x2, Pallas kernels: none -> 106 us  [the longest x1 76.4 us: split_shards(): pl.pallas_call(functools.partial(gather_kernel, n), out_shape=(jax.ShapeD...]
    reduce_scatter x2 -> x0, waiting for transfers between devices: 42.9 us -> none  [the longest x1 36.4 us: shards(): lax.psum_scatter(project_in().astype(jnp.bfloat16), 'fs', scatter_dimensi...]
    all_gather x4 -> x0, waiting for transfers between devices: 26.7 us -> none  [the longest x1 26.6 us: shards(): lax.all_gather(attn_out_weight, 'sp', axis=1, tiled=True)]
    dot_general x14 -> x6, matrix products: 23.6 us -> 11.9 us  [the longest x1 3.23 us: split_shards(): jnp.einsum('thr,jr->htj', query_rot, key_rot, preferred_element_type=f32)]
    all_to_all x1 -> x0, blocking collectives: 11 us -> none  [shards(): lax.all_to_all(outgoing, 'fs', split_axis=0, concat_axis=2, tiled=True)]
    convert_element_type x6 -> x4, other arithmetic: 6.75 us -> 0.33 us  [the longest x1 0.13 us: split_shards(): conv_y = (gate_b * convolved).astype(bf16)]
    unnamed x37 -> x26, local copies, waits for them, and re-layouts: 3.85 us -> 10.3 us
  transfers between devices with their start and end apart: 7 -> 0, of which waited for: 3 -> 0; matrix products, arithmetic and copies ran while one was open for 8% -> 0% of each run, Pallas kernels for 0% -> 0%
where the time goes in v1:
time: 138 us; the launch traced here: 136 us
  Pallas kernels  106 us (77%)
  local copies, waits for them, and re-layouts  15 us (11%)
  matrix products  11.9 us (9%)
  other arithmetic  3.49 us (3%)
    pallas_call x1, Pallas kernels, split_shards(): pl.pallas_call(functools.partial(gather_kernel, n), out_shape=(jax.ShapeD...  76.4 us
    pallas_call x1, Pallas kernels, split_shards(): pl.pallas_call(functools.partial(reduce_kernel, n), out_shape=jax.ShapeDt...  29.2 us
    unnamed x26, local copies, waits for them, and re-layouts  10.3 us
    dot_general x1, matrix products, split_shards(): jnp.einsum('thr,jr->htj', query_rot, key_rot, preferred_element_type=f32)  3.23 us
    dot_general x1, matrix products, split_shards(): jnp.einsum('thn,jhn->htj', query_nope, keys, preferred_element_type=f32)  3.02 us
    dot_general x1, matrix products, split_shards(): part = jnp.dot(mixed_y, wout, preferred_element_type=f32).astype(bf16)  2.97 us

profile of v1, /device:TPU:0, one launch (start us, length us, event | category | flops | bytes accessed | tf_op | source)
XLA Modules:
  0.0 136.1 jit_solution(13591615137537914587)
XLA Ops:
  0.0 0.8 reshape.139.gain
  0.8 1.2 copy.36.krw
  2.0 1.0 copy-done.1
  3.0 0.9 copy-done.2
  4.0 0.9 copy-done.3
  4.9 0.9 copy-done.4
  5.8 0.9 copy-done.5
  6.7 0.9 copy-done.6
  7.6 0.9 copy-done.7
  8.5 0.9 copy-done.8
  9.4 0.9 copy-done.9
  10.3 76.4 %gather_project.1 = (bf16[640,768]{1,0:T(8,128)(2,1)S(1)}, bf16[640,512]{1,0:T(8,128)(2,1)S(1)}, f32[640,64]{1,0:T(8,128)S(1)}, bf16[384,2048]{1,0:T(8,128)(2,1)S(1)}) custom-call(bf16[1,160,1024]{2,1,0:T(8,128)(2,1)S(1)} %copy-done.1, f32[2,1024]{1,0:T(2,128)S(1)} %reshape.139.gain, bf16[128,512]{1,0:T(8,128)(2,1)S(1)} %copy-done.4, ...), custom_call_target="tpu_custom_call" | custom-call | tf_op jit(solution)/shard_map/gather_project/pallas_call | solution.py:670
  86.7 2.1 %fusion.26 = (f32[640,32]{1,0:T(8,128)}, f32[640,32]{1,0:T(8,128)}, bf16[640,32]{1,0:T(8,128)(2,1)S(1)}, bf16[640,32]{1,0:T(8,128)(2,1)}) fusion(f32[32]{0:T(128)S(1)} %multiply_power_fusion, f32[640,64]{1,0:T(8,128)S(1)} %get-tuple-element.11), kind=kLoop, calls=%fused_computation.37 | loop fusion | flops 184320 | bytes 409728 | tf_op jit(solution)/shard_map/cos | solution.py:37
  89.0 1.1 copy.42
  90.1 1.1 copy.41
  91.3 3.2 %fusion.31 = f32[640,640,2]{1,0,2:T(8,128)} fusion(bf16[640,32]{1,0:T(8,128)(2,1)S(1)} %get-tuple-element.22, bf16[640,32]{1,0:T(8,128)(2,1)} %get-tuple-element.23, bf16[640,2,32]{0,2,1:T(8,128)(2,1)S(1)} %get-tuple-element.14, bf16[640,2,32]{0,2,1:T(8,128)(2,1)S(1)} %get-tuple-element.13), kind=kOutput, calls=%fused_computation.44 | convolution fusion | flops 105349120 | bytes 3522560 | tf_op jit(solution)/shard_map/thr,jr->htj/dot_general | solution.py:736
  95.6 3.0 %fusion.44 = (f32[2,640]{1,0:T(2,128)S(1)}, f32[2,640,640]{1,2,0:T(8,128)S(1)}) fusion(f32[640,640,2]{1,0,2:T(8,128)} %fusion.31, bf16[640,2,128]{0,2,1:T(8,128)(2,1)S(1)} %bitcast.41, pred[640,640]{0,1:T(8,128)(4,1)S(1)} %broadcast_compare_fusion, bf16[640,768]{1,0:T(8,128)(2,1)S(1)} %get-tuple-element.9), kind=kOutput, calls=%fused_computation.72 | convolution fusion | flops 212990720 | bytes 7623680 | tf_op jit(solution)/shard_map/thn,jhn->htj/dot_general | solution.py:735
  99.1 1.5 %convolution_convert_fusion.2 = bf16[640,256]{0,1:T(8,128)(2,1)S(1)} fusion(bf16[512,1024]{1,0:T(8,128)(2,1)} %param.28, s32[]{:T(128)S(6)} %select_n.26, bf16[640,512]{1,0:T(8,128)(2,1)S(1)} %get-tuple-element.10, f32[512]{0:T(512)S(1)} %copy-done.11, f32[640]{0:T(1024)S(1)} %add_rsqrt_fusion.1), kind=kOutput, calls=%fused_computation.17 | convolution fusion | flops 169246720 | bytes 1249796 | tf_op jit(solution)/shard_map/dot_general | solution.py:733
  100.5 0.7 multiply_reduce_fusion
  101.3 0.8 dynamic-slice_bitcast_fusion
  102.3 0.7 constant_dynamic-slice_fusion
  103.3 3.0 %convolution_convert_fusion.part = bf16[640,2048]{1,0:T(8,128)(2,1)S(1)} fusion(bf16[384,2048]{1,0:T(8,128)(2,1)} %copy-done.10, bf16[640,256]{0,1:T(8,128)(2,1)S(1)} %bitcast.42, bf16[640,128]{0,1:T(8,128)(2,1)S(1)} %copy.45), kind=kOutput, calls=%fused_computation.4 | convolution fusion | flops 1008926720 | bytes 4685824 | tf_op jit(solution)/shard_map/dot_general | solution.py:747
  106.2 29.2 %reduce_partials.1 = bf16[80,2048]{1,0:T(8,128)(2,1)S(1)} custom-call(bf16[640,2048]{1,0:T(8,128)(2,1)S(1)} %convolution_convert_fusion.part), custom_call_target="tpu_custom_call" | custom-call | tf_op jit(solution)/shard_map/reduce_partials/pallas_call | solution.py:749
  135.4 0.7 copy.58
  (32 shorter events, 2.3 us)
Async XLA Ops:
  0.0 94.7 %copy-start = (bf16[512,1024]{1,0:T(8,128)(2,1)S(1)}, bf16[512,1024]{1,0:T(8,128)(2,1)}, u32[]{:S(2)}) copy-start(bf16[512,1024]{1,0:T(8,128)(2,1)} %param.27) | copy-start | bytes 3145732
  2.0 1.0 copy-start.1
  3.0 0.9 copy-start.2
  4.0 0.9 copy-start.3
  4.9 0.9 copy-start.4
  5.8 0.9 copy-start.5
  6.7 0.9 copy-start.6
  7.6 0.9 copy-start.7
  8.5 0.9 copy-start.8
  9.4 0.9 copy-start.9
  86.7 2.1 %copy-start.10 = (bf16[384,2048]{1,0:T(8,128)(2,1)}, bf16[384,2048]{1,0:T(8,128)(2,1)S(1)}, u32[]{:S(2)}) copy-start(bf16[384,2048]{1,0:T(8,128)(2,1)S(1)} %get-tuple-element.12) | copy-start | bytes 4718596
  91.2 3.5 %copy-start.11 = (f32[512]{0:T(512)S(1)}, f32[512]{0:T(512)}, u32[]{:S(2)}) copy-start(f32[512]{0:T(512)} %param.26) | copy-start | bytes 6148

commit v2 on v1

--- a/solution.py
+++ b/solution.py
@@ -1,4 +1,5 @@
 import functools
+import math
 
 import jax
 import jax.numpy as jnp
@@ -267,32 +268,57 @@
     pl.semaphore_wait(barrier, len(devices))
 
 
-def gather_kernel(
+def layer_kernel(
     n,
+    turns,
     tok_in,
-    gain,
+    gain_in,
     cb,
     cc,
     cv,
+    taps_in,
     qw,
     qr,
     lw,
-    krw,
+    krw_in,
+    lat_gain_in,
+    key_up_in,
+    value_up_in,
+    head_gain_in,
     co,
     ao,
-    proj_out,
-    lat_out,
-    krot_out,
-    wout,
+    out,
     tok,
     normed,
     win,
+    wout,
     lat,
+    gain,
+    krw,
+    taps,
+    lat_gain,
+    key_up,
+    value_up,
+    head_gain,
+    conv_y,
+    q_nope,
+    q_rot,
+    keys,
+    values,
+    cosine,
+    sine,
+    part,
+    pair,
+    moving,
+    fetched,
     wsem,
     lsem,
     tsem,
     psem,
     latsem,
+    ssem,
+    pairsem,
+    zsem,
 ):
     here = Place()
     z, f, c = here.z, here.f, here.c
@@ -402,6 +428,25 @@
     def can(sign):
         return (z + sign >= 0) & (z + sign < n)
 
+    channels = widths[0]
+    heads = widths[3] // NOPE
+    rot_w = widths[4]
+    share = tr // 2
+
+    def columns_of(array, width):
+        return array.at[:, pl.ds(pl.multiple_of(z * width, width), width)]
+
+    small = [
+        (gain_in, gain),
+        (krw_in, krw.at[0:ROPE, :]),
+        (krw_in, krw.at[ROPE : 2 * ROPE, :]),
+        (columns_of(taps_in, channels), taps),
+        (lat_gain_in, lat_gain),
+        (columns_of(key_up_in, heads * NOPE), key_up),
+        (columns_of(value_up_in, heads * VD), value_up),
+        (columns_of(head_gain_in, heads * VD), head_gain),
+    ]
+
     send_own(0)
     for distance, sign in steps[:2]:
         send_z(0, distance, sign)
@@ -411,6 +456,8 @@
         pl.when(can(sign))(lambda sign=sign: tok_copy(z, sign, 0, own_tok).start())
     for distance, sign in steps[2:]:
         send_z(0, distance, sign)
+    for i, (src, dst) in enumerate(small):
+        pltpu.make_async_copy(src, dst, ssem.at[i]).start()
 
     def relay_tok(distance, sign):
         zs = z + sign * distance
@@ -422,13 +469,6 @@
                 pl.when(can(-sign))(lambda: tok_copy(zs, -sign, distance).start())
             partner_copy(zs, c).start()
 
-    for distance, sign in steps:
-        relay_z(0, distance, sign)
-        relay_tok(distance, sign)
-    send_own(1)
-    for distance, sign in steps:
-        send_z(1, distance, sign)
-
     def each_zs(fn):
         def body(i, carry):
             fn(lax.rem(z + i, n))
@@ -436,36 +476,77 @@
 
         lax.fori_loop(0, n, body, 0)
 
-    def tok_ready(zs):
-        partner_copy(zs, other).wait_recv()
-
-    each_zs(tok_ready)
-    pltpu.make_async_copy(own_tok, tok_block(c, z), lsem.at[2]).wait()
+    def at_distance(distance, fn):
+        if distance == 0:
+            fn(z)
+            return
+        for sign in (-1, 1):
+            zs = z + sign * distance
+            pl.when((zs >= 0) & (zs < n))(lambda zs=zs: fn(zs))
+
+    lane = lax.broadcasted_iota(jnp.int32, (tr, rot_w), 1)
+    quarter = lane % (ROPE // 2)
+    first_half = (lane % ROPE) < ROPE // 2
+    frequency = jnp.exp(quarter.astype(jnp.float32) * (-2.0 / ROPE * math.log(rope_theta)))
+
+    def tables(i, carry):
+        at = pl.ds(pl.multiple_of(i * tr, tr), tr)
+        position = (i * tr + lax.broadcasted_iota(jnp.int32, (tr, rot_w), 0)).astype(jnp.float32)
+        angle = position * frequency
+        cosine[at, :] = jnp.cos(angle)
+        turned = jnp.sin(angle)
+        sine[at, :] = jnp.where(first_half, -turned, turned)
+        return carry
+
+    lax.fori_loop(0, n, tables, 0)
+
+    def rotated(x, at):
+        swapped = jnp.where(
+            first_half, pltpu.roll(x, rot_w - ROPE // 2, 1), pltpu.roll(x, ROPE // 2, 1)
+        )
+        return (x * cosine[at, :] + swapped * sine[at, :]).astype(jnp.bfloat16)
+
+    for i, (src, dst) in enumerate(small):
+        pltpu.make_async_copy(src, dst, ssem.at[i]).wait()
     chunk = tr // 2
     wide = tok.shape[2]
 
-    def norm_chunk(i, carry):
-        at = pl.ds(pl.multiple_of(i * chunk, chunk), chunk)
-        first = tok[0, at, :].astype(jnp.float32)
-        second = tok[1, at, :].astype(jnp.float32)
-        mean = (
-            jnp.sum(first * first, axis=-1, keepdims=True) + jnp.sum(second * second, axis=-1, keepdims=True)
-        ) / (2 * wide)
-        scale = lax.rsqrt(mean + norm_epsilon)
-        normed[at, 0:wide] = (first * scale * gain[0, :]).astype(jnp.bfloat16)
-        normed[at, wide : 2 * wide] = (second * scale * gain[1, :]).astype(jnp.bfloat16)
-        return carry
-
-    each_zs(lambda zs: relay_plane(0, zs))
-    lax.fori_loop(0, 2 * n, norm_chunk, 0)
+    def norm_block(zs):
+        partner_copy(zs, other).wait_recv()
+
+        def norm_chunk(i, carry):
+            at = pl.ds(pl.multiple_of(zs * tr + i * chunk, chunk), chunk)
+            first = tok[0, at, :].astype(jnp.float32)
+            second = tok[1, at, :].astype(jnp.float32)
+            mean = (
+                jnp.sum(first * first, axis=-1, keepdims=True)
+                + jnp.sum(second * second, axis=-1, keepdims=True)
+            ) / (2 * wide)
+            scale = lax.rsqrt(mean + norm_epsilon)
+            normed[at, 0:wide] = (first * scale * gain[0:1, 0:wide]).astype(jnp.bfloat16)
+            normed[at, wide : 2 * wide] = (second * scale * gain[0:1, wide : 2 * wide]).astype(jnp.bfloat16)
+            return carry
+
+        lax.fori_loop(0, 2, norm_chunk, 0)
+
+    pltpu.make_async_copy(own_tok, tok_block(c, z), lsem.at[2]).wait()
+    for distance in range(1, n):
+        for sign in (-1, 1):
+            relay_z(0, distance, sign)
+        for sign in (-1, 1):
+            relay_tok(distance, sign)
+        at_distance(distance - 1, lambda zs: relay_plane(0, zs))
+        at_distance(distance - 1, norm_block)
+    send_own(1)
     for distance, sign in steps:
-        relay_z(1, distance, sign)
+        send_z(1, distance, sign)
+    at_distance(n - 1, lambda zs: relay_plane(0, zs))
+    at_distance(n - 1, norm_block)
 
     def relay_done(kind, zs):
         plane_copy(kind, zs, 6, flip(fx, 2), fx).wait_recv()
 
-    for src, dst in pieces(0, z)[:1]:
-        pltpu.make_async_copy(in_block(z, f), in_block(z, f), lsem.at[0]).wait()
+    pltpu.make_async_copy(in_block(z, f), in_block(z, f), lsem.at[0]).wait()
     each_zs(lambda zs: relay_done(0, zs))
 
     def lat_block(zs, owner):
@@ -489,33 +570,183 @@
     for j in range(1, n):
         lat_copy(lax.rem(z + j, n)).start()
     lat_partner(z, c).start()
-    each_zs(lambda zs: relay_plane(1, zs))
+    for distance in range(1, n):
+        for sign in (-1, 1):
+            relay_z(1, distance, sign)
+        at_distance(distance - 1, lambda zs: relay_plane(1, zs))
 
     def project(i, carry):
         at = pl.ds(pl.multiple_of(i * tr, tr), tr)
-        proj_out[at, :] = jnp.dot(
-            normed[at, :], win[:, 0:proj_w], preferred_element_type=jnp.float32
-        ).astype(jnp.bfloat16)
-        krot_out[at, :] = jnp.dot(normed[at, :], krw[...], preferred_element_type=jnp.float32)
-        return carry
-
-    lax.fori_loop(0, n, project, 0)
+        block = normed[at, :]
+        joined = jnp.dot(block, win[:, 0:proj_w], preferred_element_type=jnp.float32)
+        gates = joined[:, 0 : 3 * channels].astype(jnp.bfloat16).astype(jnp.float32)
+        gate_b = gates[:, 0:channels]
+        product = (
+            (gates[:, channels : 2 * channels] * gates[:, 2 * channels : 3 * channels])
+            .astype(jnp.bfloat16)
+            .astype(jnp.float32)
+        )
+        row = lax.broadcasted_iota(jnp.int32, (tr, channels), 0)
+        older, newer = carry
+        once = jnp.where(row == 0, newer, pltpu.roll(product, 1, 0))
+        twice = jnp.where(row == 0, older, jnp.where(row == 1, newer, pltpu.roll(product, 2, 0)))
+        convolved = taps[0:1, :] * twice + taps[1:2, :] * once + taps[2:3, :] * product
+        conv_y[at, :] = (gate_b * convolved).astype(jnp.bfloat16)
+        start = 3 * channels
+        q_nope[at, :] = joined[:, start : start + heads * NOPE].astype(jnp.bfloat16)
+        q_rot[at, :] = rotated(joined[:, start + heads * NOPE :], at)
+        key_raw = lax.dot_general(
+            block, krw[...], (((1,), (1,)), ((), ())), preferred_element_type=jnp.float32
+        )
+        key_rot = rotated(key_raw, at)
+        for h in range(heads):
+            keys[h, at, NOPE:] = key_rot
+        return product[tr - 2 : tr - 1, :], product[tr - 1 : tr, :]
+
+    nothing = jnp.zeros((1, channels), jnp.float32)
+    lax.fori_loop(0, n, project, (nothing, nothing))
+    at_distance(n - 1, lambda zs: relay_plane(1, zs))
     for j in range(1, n):
         zs = lax.rem(z + j, n)
         lat_arrival(zs).wait_recv()
         lat_partner(zs, c).start()
     each_zs(lambda zs: lat_partner(zs, other).wait_recv())
-    for k in range(n):
-        lat_out[:, k * lat_w : (k + 1) * lat_w] = lat[k]
-
+
+    def expand(i, carry):
+        at = pl.ds(pl.multiple_of(i * tr, tr), tr)
+        raw = jnp.concatenate([lat[k, at, :] for k in range(n)], axis=1).astype(jnp.float32)
+        mean = jnp.mean(raw * raw, axis=-1, keepdims=True)
+        low = (raw * lax.rsqrt(mean + norm_epsilon) * lat_gain[0:1, :]).astype(jnp.bfloat16)
+        wide_keys = jnp.dot(low, key_up[...], preferred_element_type=jnp.float32).astype(jnp.bfloat16)
+        for h in range(heads):
+            keys[h, at, 0:NOPE] = wide_keys[:, h * NOPE : (h + 1) * NOPE]
+        values[at, :] = jnp.dot(low, value_up[...], preferred_element_type=jnp.float32).astype(jnp.bfloat16)
+        return carry
+
+    lax.fori_loop(0, n, expand, 0)
     pltpu.make_async_copy(out_block(z, f), out_block(z, f), lsem.at[1]).wait()
     each_zs(lambda zs: relay_done(1, zs))
+
+    shift = SEG.bit_length() - 1
+    row_index = lax.broadcasted_iota(jnp.int32, (tr, length), 0)
+    key_segment = jnp.right_shift(lax.broadcasted_iota(jnp.int32, (tr, length), 1), shift)
+    own_lanes = lane // ROPE
+
+    def block_output(dest):
+        at = pl.ds(pl.multiple_of(dest * tr, tr), tr)
+        allowed = key_segment <= jnp.right_shift(row_index + dest * tr, shift)
+        outputs = [conv_y[at, :]]
+        rot = q_rot[at, :]
+        for h in range(heads):
+            query = jnp.concatenate(
+                [
+                    q_nope[at, h * NOPE : (h + 1) * NOPE],
+                    jnp.where(own_lanes == h, rot, jnp.zeros_like(rot)),
+                ],
+                axis=1,
+            )
+            scores = lax.dot_general(
+                query, keys[h], (((1,), (1,)), ((), ())), preferred_element_type=jnp.float32
+            ) * (NOPE + ROPE) ** (-0.5)
+            scores = jnp.where(allowed, scores, -1e30)
+            weights = jnp.exp(scores - jnp.max(scores, axis=-1, keepdims=True))
+            denom = jnp.sum(weights, axis=-1, keepdims=True)
+            head_out = (
+                jnp.dot(
+                    weights.astype(jnp.bfloat16),
+                    values[:, h * VD : (h + 1) * VD],
+                    preferred_element_type=jnp.float32,
+                )
+                / denom
+            )
+            mean = jnp.mean(head_out * head_out, axis=-1, keepdims=True)
+            gained = head_out * lax.rsqrt(mean + norm_epsilon) * head_gain[0:1, h * VD : (h + 1) * VD]
+            outputs.append(gained.astype(jnp.bfloat16))
+        mixed = jnp.concatenate(outputs, axis=1)
+        part[dest] = jnp.dot(mixed, wout[...], preferred_element_type=jnp.float32).astype(jnp.bfloat16)
+
+    def part_rows(dest, core):
+        return part.at[dest, pl.ds(pl.multiple_of(core * share, share), share), :]
+
+    def pair_copy(dest):
+        return remote(
+            part_rows(dest, other), pair.at[dest], pairsem.at[0, dest], pairsem.at[1, dest], here.to(c=other)
+        )
+
+    def line_copy(d, dest):
+        return remote(
+            moving.at[dest],
+            fetched.at[d, dest],
+            zsem.at[d, 0, dest],
+            zsem.at[d, 1, dest],
+            here.to(z=z + 2 * d - 1),
+        )
+
+    def turn_of(t):
+        dest = jnp.int32(0)
+        for zz in range(n):
+            for tt in range(n):
+                dest = jnp.where((z == zz) & (t == tt), turns[zz][tt], dest)
+        return dest
+
+    def summed(dest):
+        kept = part[dest, pl.ds(pl.multiple_of(c * share, share), share), :]
+        return kept.astype(jnp.float32) + pair[dest].astype(jnp.float32)
+
+    def pass_on(dest):
+        d = jnp.where(dest > z, 1, 0)
+        before = z - (2 * d - 1)
+        has = (before >= 0) & (before < n)
+        pair_copy(dest).wait_recv()
+
+        @pl.when(has)
+        def _():
+            line_copy(d, dest).wait_recv()
+            moving[dest] = (summed(dest) + fetched[d, dest].astype(jnp.float32)).astype(jnp.bfloat16)
+
+        @pl.when(jnp.logical_not(has))
+        def _():
+            moving[dest] = summed(dest).astype(jnp.bfloat16)
+
+        line_copy(d, dest).start()
+
+    def turn(t, carry):
+        dest = turn_of(t)
+        block_output(dest)
+        pair_copy(dest).start()
+        pl.when(t >= 1)(lambda: pass_on(turn_of(t - 1)))
+        return carry
+
+    lax.fori_loop(0, n, turn, 0)
+    pair_copy(z).wait_recv()
+    low, high = z > 0, z < n - 1
+
+    @pl.when(low)
+    def _():
+        line_copy(1, z).wait_recv()
+
+    @pl.when(high)
+    def _():
+        line_copy(0, z).wait_recv()
+
+    @pl.when(low & high)
+    def _():
+        out[...] = (
+            summed(z) + fetched[1, z].astype(jnp.float32) + fetched[0, z].astype(jnp.float32)
+        ).astype(jnp.bfloat16)
+
+    @pl.when(jnp.logical_not(low & high))
+    def _():
+        d = jnp.where(low, 1, 0)
+        out[...] = (summed(z) + fetched[d, z].astype(jnp.float32)).astype(jnp.bfloat16)
+
     for j in range(1, n):
         zs = lax.rem(z + j, n)
         for kind in (0, 1):
             block = blocks[kind](zs, f)
             remote(block, block, wsem.at[kind, 0, zs], wsem.at[kind, 1, zs], here.to(z=zs)).wait_send()
         lat_copy(zs).wait_send()
+        line_copy(jnp.where(zs > z, 1, 0), zs).wait_send()
 
     def sent(zs):
         for kind in (0, 1):
@@ -524,6 +755,7 @@
             plane_copy(kind, zs, 6, fx, fy).wait_send()
         partner_copy(zs, c).wait_send()
         lat_partner(zs, c).wait_send()
+        pair_copy(zs).wait_send()
 
     each_zs(sent)
     for sign in (-1, 1):
@@ -533,104 +765,6 @@
             pl.when((zs >= 0) & (zs < n) & can(sign))(
                 lambda sign=sign, distance=distance: tok_copy(z, sign, distance).wait_send()
             )
-
-
-def reduce_kernel(n, part, out, own, pair, moving, fetched, csem, psem, zsem):
-    here = Place()
-    z, c = here.z, here.c
-    other = 1 - c
-    share = out.shape[0]
-    greet(
-        [here.to(c=other)]
-        + [here.to(z=lax.rem(z + 1, n)), here.to(z=lax.rem(z + n - 1, n))]
-    )
-
-    def rows(zs, core):
-        return part.at[pl.ds(pl.multiple_of((2 * zs + core) * share, share), share), :]
-
-    def pair_copy(zs):
-        return remote(rows(zs, other), pair.at[zs], psem.at[0, zs], psem.at[1, zs], here.to(c=other))
-
-    def own_copy(zs):
-        return pltpu.make_async_copy(rows(zs, c), own.at[zs], csem.at[zs])
-
-    order = [j for j in range(n - 1, -1, -1)]
-
-    def line_copy(d, dest):
-        return remote(
-            moving.at[d, dest],
-            fetched.at[d, dest],
-            zsem.at[d, 0, dest],
-            zsem.at[d, 1, dest],
-            here.to(z=z + 2 * d - 1),
-        )
-
-    turns = [(far, d) for far in range(n - 1, -1, -1) for d in (0, 1)]
-    for far, d in turns:
-        dest = z + (2 * d - 1) * far
-        if far == 0 and d == 1:
-            continue
-
-        @pl.when((dest >= 0) & (dest < n))
-        def _():
-            pair_copy(dest).start()
-            own_copy(dest).start()
-
-    def summed(dest):
-        return own[dest].astype(jnp.float32) + pair[dest].astype(jnp.float32)
-
-    for far, d in turns:
-        dest = z + (2 * d - 1) * far
-        if far == 0:
-            continue
-
-        @pl.when((dest >= 0) & (dest < n))
-        def _():
-            own_copy(dest).wait()
-            pair_copy(dest).wait_recv()
-            before = z - (2 * d - 1)
-            has = (before >= 0) & (before < n)
-
-            @pl.when(has)
-            def _():
-                line_copy(d, dest).wait_recv()
-                moving[d, dest] = (summed(dest) + fetched[d, dest].astype(jnp.float32)).astype(jnp.bfloat16)
-
-            @pl.when(jnp.logical_not(has))
-            def _():
-                moving[d, dest] = summed(dest).astype(jnp.bfloat16)
-
-            line_copy(d, dest).start()
-
-    own_copy(z).wait()
-    pair_copy(z).wait_recv()
-    low, high = z > 0, z < n - 1
-
-    @pl.when(low)
-    def _():
-        line_copy(1, z).wait_recv()
-
-    @pl.when(high)
-    def _():
-        line_copy(0, z).wait_recv()
-
-    result = summed(z)
-    from_low = fetched[1, z].astype(jnp.float32)
-    from_high = fetched[0, z].astype(jnp.float32)
-    zero = jnp.zeros_like(result)
-    result = result + jnp.where(low, from_low, zero) + jnp.where(high, from_high, zero)
-    out[...] = result.astype(jnp.bfloat16)
-
-    for far, d in turns:
-        dest = z + (2 * d - 1) * far
-        if far == 0 and d == 1:
-            continue
-
-        @pl.when((dest >= 0) & (dest < n))
-        def _():
-            pair_copy(dest).wait_send()
-            if far:
-                line_copy(d, dest).wait_send()
 
 
 def split_shards(
@@ -652,7 +786,6 @@
     attn_out_weight,
 ):
     n = lax.axis_size("sp")
-    z = lax.axis_index("sp")
     tr = tokens.shape[1]
     wide = tokens.shape[2]
     length = n * tr
@@ -663,108 +796,70 @@
     proj_w = 3 * channels + heads * (NOPE + ROPE)
     out_rows = (conv_out_weight.shape[0] + attn_out_weight.shape[0]) // n
     columns = attn_out_weight.shape[1] * n * 4
-    bf16 = jnp.bfloat16
-    vmem = pl.BlockSpec(memory_space=pltpu.VMEM)
-    anywhere = pl.BlockSpec(memory_space=pl.ANY)
+    share = tr // 2
+    bf16, f32 = jnp.bfloat16, jnp.float32
+    turns = [sorted(range(n), key=lambda dest: (-abs(dest - at), dest)) for at in range(n)]
     dma = pltpu.SemaphoreType.DMA
-    proj, lat_raw, krot_raw, wout = pl.pallas_call(
-        functools.partial(gather_kernel, n),
-        out_shape=(
-            jax.ShapeDtypeStruct((length, proj_w), bf16),
-            jax.ShapeDtypeStruct((length, n * lat_w), bf16),
-            jax.ShapeDtypeStruct((length, ROPE), jnp.float32),
-            jax.ShapeDtypeStruct((out_rows, columns), bf16),
-        ),
-        in_specs=[anywhere, vmem] + [anywhere] * 6 + [vmem] + [anywhere] * 2,
-        out_specs=(vmem, vmem, vmem, anywhere),
+    result = pl.pallas_call(
+        functools.partial(layer_kernel, n, turns),
+        out_shape=jax.ShapeDtypeStruct((share, columns), bf16),
+        in_specs=[pl.BlockSpec(memory_space=pltpu.HBM)] * 16,
+        out_specs=pl.BlockSpec(memory_space=pltpu.VMEM),
         scratch_shapes=[
             pltpu.VMEM((2, length, wide), bf16),
             pltpu.VMEM((length, features), bf16),
             pltpu.VMEM((features, proj_w + lat_w), bf16),
+            pltpu.VMEM((out_rows, columns), bf16),
             pltpu.VMEM((n, length, lat_w), bf16),
+            pltpu.VMEM((8, features), f32),
+            pltpu.VMEM((2 * ROPE, features), bf16),
+            pltpu.VMEM((8, channels), f32),
+            pltpu.VMEM((8, n * lat_w), f32),
+            pltpu.VMEM((n * lat_w, heads * NOPE), bf16),
+            pltpu.VMEM((n * lat_w, heads * VD), bf16),
+            pltpu.VMEM((8, heads * VD), f32),
+            pltpu.VMEM((length, channels), bf16),
+            pltpu.VMEM((length, heads * NOPE), bf16),
+            pltpu.VMEM((length, heads * ROPE), bf16),
+            pltpu.VMEM((heads, length, NOPE + 2 * ROPE), bf16),
+            pltpu.VMEM((length, heads * VD), bf16),
+            pltpu.VMEM((length, heads * ROPE), f32),
+            pltpu.VMEM((length, heads * ROPE), f32),
+            pltpu.VMEM((n, tr, columns), bf16),
+            pltpu.VMEM((n, share, columns), bf16),
+            pltpu.VMEM((n, share, columns), bf16),
+            pltpu.VMEM((2, n, share, columns), bf16),
             dma((2, 8, n)),
             dma((3,)),
             dma((2, 2, n)),
             dma((2, n)),
             dma((4, n)),
-        ],
-        compiler_params=pltpu.CompilerParams(
-            collective_id=0, has_side_effects=True, vmem_limit_bytes=48 * 1024 * 1024
-        ),
-        name="gather_project",
-    )(
-        tokens,
-        mix_gain.reshape(2, wide),
-        conv_b_weight,
-        conv_c_weight,
-        conv_v_weight,
-        query_weight,
-        query_rope_weight,
-        latent_weight,
-        key_rope_weight,
-        conv_out_weight,
-        attn_out_weight,
-    )
-    f32 = jnp.float32
-
-    def mine(array, axis):
-        width = array.shape[axis] // n
-        return lax.dynamic_slice_in_dim(array, z * width, width, axis)
-
-    taps = mine(conv_taps, 1)
-    key_up = mine(key_up_weight, 1)
-    value_up = mine(value_up_weight, 1)
-    gain = mine(head_gain, 0).reshape(heads, VD)
-    cosine, sine = rope_tables(jnp.arange(length, dtype=f32))
-    gate_b, gate_c, values_v = (proj[:, i * channels : (i + 1) * channels].astype(f32) for i in range(3))
-    at = 3 * channels
-    query_nope = proj[:, at : at + heads * NOPE].reshape(length, heads, NOPE)
-    at = at + heads * NOPE
-    query_rot = rotate(
-        proj[:, at:].astype(f32).reshape(length, heads, ROPE), cosine[:, None, :], sine[:, None, :]
-    ).astype(bf16)
-    product = (gate_c * values_v).astype(bf16)
-    padded = jnp.concatenate([jnp.zeros((2, channels), bf16), product], axis=0).astype(f32)
-    convolved = taps[0] * padded[0:length] + taps[1] * padded[1 : length + 1] + taps[2] * padded[2 : length + 2]
-    conv_y = (gate_b * convolved).astype(bf16)
-    latent = rms_scale(lat_raw.astype(f32), latent_gain).astype(bf16)
-    key_rot = rotate(krot_raw, cosine, sine).astype(bf16)
-    keys = jnp.dot(latent, key_up, preferred_element_type=f32).astype(bf16).reshape(length, heads, NOPE)
-    values = jnp.dot(latent, value_up, preferred_element_type=f32).astype(bf16).reshape(length, heads, VD)
-    scores = (
-        jnp.einsum("thn,jhn->htj", query_nope, keys, preferred_element_type=f32)
-        + jnp.einsum("thr,jr->htj", query_rot, key_rot, preferred_element_type=f32)
-    ) * (NOPE + ROPE) ** (-0.5)
-    segment = jnp.arange(length, dtype=jnp.int32) // SEG
-    allowed = segment[None, None, :] <= segment[None, :, None]
-    scores = jnp.where(allowed, scores, -1e30)
-    weights = jnp.exp(scores - jnp.max(scores, axis=-1, keepdims=True))
-    denom = jnp.sum(weights, axis=-1)
-    head_out = jnp.einsum("htj,jhv->thv", weights.astype(bf16), values, preferred_element_type=f32)
-    head_out = head_out / denom.T[:, :, None]
-    attn_y = rms_scale(head_out, gain).astype(bf16).reshape(length, heads * VD)
-    mixed_y = jnp.concatenate([conv_y, attn_y], axis=1)
-    part = jnp.dot(mixed_y, wout, preferred_element_type=f32).astype(bf16)
-    share = tr // 2
-    result = pl.pallas_call(
-        functools.partial(reduce_kernel, n),
-        out_shape=jax.ShapeDtypeStruct((share, columns), bf16),
-        in_specs=[anywhere],
-        out_specs=vmem,
-        scratch_shapes=[
-            pltpu.VMEM((n, share, columns), bf16),
-            pltpu.VMEM((n, share, columns), bf16),
-            pltpu.VMEM((2, n, share, columns), bf16),
-            pltpu.VMEM((2, n, share, columns), bf16),
-            dma((n,)),
+            dma((8,)),
             dma((2, n)),
             dma((2, 2, n)),
         ],
         compiler_params=pltpu.CompilerParams(
-            collective_id=1, has_side_effects=True, vmem_limit_bytes=32 * 1024 * 1024
+            collective_id=0, has_side_effects=True, vmem_limit_bytes=56 * 1024 * 1024
         ),
-        name="reduce_partials",
-    )(part)
+        name="whole_layer",
+    )(
+        tokens,
+        jnp.broadcast_to(mix_gain, (8, features)),
+        conv_b_weight,
+        conv_c_weight,
+        conv_v_weight,
+        jnp.concatenate([conv_taps, jnp.zeros((8 - conv_taps.shape[0], conv_taps.shape[1]), f32)], axis=0),
+        query_weight,
+        query_rope_weight,
+        latent_weight,
+        key_rope_weight.T,
+        jnp.broadcast_to(latent_gain, (8, n * lat_w)),
+        key_up_weight,
+        value_up_weight,
+        jnp.broadcast_to(head_gain, (8, head_gain.shape[0])),
+        conv_out_weight,
+        attn_out_weight,
+    )
     return result[None]
 
 
@@ -777,7 +872,7 @@
     n = lax.axis_size("sp")
     conv, query, rope, low_rank = (arrays[i].shape[1] for i in (2, 6, 7, 8))
     heads = query // NOPE
-    even = heads % n == 0 and all(w % (128 * n) == 0 for w in (conv, query, rope, low_rank))
+    even = heads == n * 128 // ROPE and all(w % (128 * n) == 0 for w in (conv, query, rope, low_rank))
     if even and arrays[0].shape[1] % 32 == 0 and arrays[15].shape[1] % 128 == 0:
         return split_shards(*arrays)
     return general_shards(*arrays)

time: 138 us -> 110 us (0.80); the launches traced: 136 us -> 110 us
  matrix products: 11.9 us -> 0 us
  local copies, waits for them, and re-layouts: 15 us -> 5.07 us
  other arithmetic: 3.49 us -> 0 us
    dot_general x6 -> x0, matrix products: 11.9 us -> none  [the longest x1 3.23 us: split_shards(): jnp.einsum('thr,jr->htj', query_rot, key_rot, preferred_element_type=f32)]
    unnamed x26 -> x7, local copies, waits for them, and re-layouts: 10.3 us -> 1.91 us
    cos x1 -> x0, other arithmetic: 2.1 us -> none  [rope_tables(): return (jnp.cos(angles), jnp.sin(angles))]
    broadcast_in_dim x0 -> x3, local copies, waits for them, and re-layouts: none -> 1.84 us  [the longest x1 0.63 us: split_shards(): jnp.broadcast_to(mix_gain, (8, features))]
    pallas_call x2 -> x1, Pallas kernels: 106 us -> 105 us  [split_shards(): pl.pallas_call(functools.partial(layer_kernel, n, turns), out_shape=jax.S...]
where the time goes in v2:
time: 110 us
  Pallas kernels  105 us (95%)
  local copies, waits for them, and re-layouts  5.07 us (5%)
    pallas_call x1, Pallas kernels, split_shards(): pl.pallas_call(functools.partial(layer_kernel, n, turns), out_shape=jax.S...  105 us

profile of v2, /device:TPU:0, one launch (start us, length us, event | category | flops | bytes accessed | tf_op | source)
XLA Modules:
  0.0 109.9 jit_solution(16037513039537970082)
XLA Ops:
  0.0 0.0 copy-start.2
  0.0 1.3 %concatenate.3.taps_in = f32[8,512]{1,0:T(8,128)} pad(f32[3,512]{1,0:T(4,128)} %param.21, f32[]{:T(128)} %constant.0.clone.1), padding=0_5x0_0 | pad | bytes 22532 | tf_op jit(solution)/shard_map/concatenate | solution.py:851
  1.3 0.0 copy-done.2
  1.3 0.0 copy-start.1
  1.3 0.6 broadcast_in_dim.14.lat_gain_in
  1.9 0.1 copy-done.1
  2.0 0.0 copy-start
  2.0 0.6 broadcast_in_dim.15.head_gain_in
  2.6 0.1 copy-done
  2.7 0.6 broadcast_in_dim.13.gain_in
  3.4 104.8 %whole_layer.1 = bf16[80,2048]{1,0:T(8,128)(2,1)} custom-call(bf16[1,160,1024]{2,1,0:T(8,128)(2,1)} %tok_in.1, f32[8,2048]{1,0:T(8,128)} %broadcast_in_dim.13.gain_in, bf16[128,512]{1,0:T(8,128)(2,1)} %cb.1, bf16[128,512]{1,0:T(8,128)(2,1)} %cc.1, bf16[128,512]{1,0:T(8,128)(2,1)} %cv.1, f32[8,512]{1,0:T(8,128)} %concatenate.3.taps_in, bf16[128,1024]{1,0:T(8,128)(2,1)} %qw.1, ...), custom_call_target="tpu_custom_call" | custom-call | tf_op jit(solution)/shard_map/whole_layer/pallas_call | solution.py:803
  108.2 1.7 %copy.18 = bf16[1,80,2048]{2,1,0:T(8,128)(2,1)} copy(bf16[1,80,2048]{2,1,0:T(8,128)(2,1)} %bitcast.2) | data formatting | bytes 655360
Async XLA Ops:
  0.0 1.3 %copy-start.2 = (f32[512]{0:T(512)S(1)}, f32[512]{0:T(512)}, u32[]{:S(2)}) copy-start(f32[512]{0:T(512)} %param.26) | copy-start | bytes 6148
  1.3 0.7 copy-start.1
  2.0 0.7 copy-start

commit v3 on v2

--- a/solution.py
+++ b/solution.py
@@ -272,19 +272,16 @@
     n,
     turns,
     tok_in,
-    gain_in,
+    params,
     cb,
     cc,
     cv,
-    taps_in,
     qw,
     qr,
     lw,
     krw_in,
-    lat_gain_in,
     key_up_in,
     value_up_in,
-    head_gain_in,
     co,
     ao,
     out,
@@ -436,15 +433,17 @@
     def columns_of(array, width):
         return array.at[:, pl.ds(pl.multiple_of(z * width, width), width)]
 
+    low_w = n * lat_w
+    shift_by = pl.multiple_of(low_w + z * heads * VD, 128)
     small = [
-        (gain_in, gain),
+        (params, gain),
         (krw_in, krw.at[0:ROPE, :]),
         (krw_in, krw.at[ROPE : 2 * ROPE, :]),
-        (columns_of(taps_in, channels), taps),
-        (lat_gain_in, lat_gain),
+        (columns_of(params, channels), taps),
+        (params.at[:, 0:low_w], lat_gain),
         (columns_of(key_up_in, heads * NOPE), key_up),
         (columns_of(value_up_in, heads * VD), value_up),
-        (columns_of(head_gain_in, heads * VD), head_gain),
+        (params.at[:, pl.ds(shift_by, heads * VD)], head_gain),
     ]
 
     send_own(0)
@@ -590,7 +589,7 @@
         older, newer = carry
         once = jnp.where(row == 0, newer, pltpu.roll(product, 1, 0))
         twice = jnp.where(row == 0, older, jnp.where(row == 1, newer, pltpu.roll(product, 2, 0)))
-        convolved = taps[0:1, :] * twice + taps[1:2, :] * once + taps[2:3, :] * product
+        convolved = taps[2:3, :] * twice + taps[3:4, :] * once + taps[4:5, :] * product
         conv_y[at, :] = (gate_b * convolved).astype(jnp.bfloat16)
         start = 3 * channels
         q_nope[at, :] = joined[:, start : start + heads * NOPE].astype(jnp.bfloat16)
@@ -616,7 +615,7 @@
         at = pl.ds(pl.multiple_of(i * tr, tr), tr)
         raw = jnp.concatenate([lat[k, at, :] for k in range(n)], axis=1).astype(jnp.float32)
         mean = jnp.mean(raw * raw, axis=-1, keepdims=True)
-        low = (raw * lax.rsqrt(mean + norm_epsilon) * lat_gain[0:1, :]).astype(jnp.bfloat16)
+        low = (raw * lax.rsqrt(mean + norm_epsilon) * lat_gain[1:2, :]).astype(jnp.bfloat16)
         wide_keys = jnp.dot(low, key_up[...], preferred_element_type=jnp.float32).astype(jnp.bfloat16)
         for h in range(heads):
             keys[h, at, 0:NOPE] = wide_keys[:, h * NOPE : (h + 1) * NOPE]
@@ -660,7 +659,7 @@
                 / denom
             )
             mean = jnp.mean(head_out * head_out, axis=-1, keepdims=True)
-            gained = head_out * lax.rsqrt(mean + norm_epsilon) * head_gain[0:1, h * VD : (h + 1) * VD]
+            gained = head_out * lax.rsqrt(mean + norm_epsilon) * head_gain[1:2, h * VD : (h + 1) * VD]
             outputs.append(gained.astype(jnp.bfloat16))
         mixed = jnp.concatenate(outputs, axis=1)
         part[dest] = jnp.dot(mixed, wout[...], preferred_element_type=jnp.float32).astype(jnp.bfloat16)
@@ -800,10 +799,19 @@
     bf16, f32 = jnp.bfloat16, jnp.float32
     turns = [sorted(range(n), key=lambda dest: (-abs(dest - at), dest)) for at in range(n)]
     dma = pltpu.SemaphoreType.DMA
+
+    def row(values):
+        return jnp.pad(values, (0, features - values.shape[0]))[None]
+
+    gains = row(jnp.concatenate([latent_gain, head_gain]))
+    spare = 8 - 2 - conv_taps.shape[0]
+    params = jnp.concatenate(
+        [mix_gain[None], gains, jnp.pad(conv_taps, ((0, spare), (0, features - conv_taps.shape[1])))], axis=0
+    )
     result = pl.pallas_call(
         functools.partial(layer_kernel, n, turns),
         out_shape=jax.ShapeDtypeStruct((share, columns), bf16),
-        in_specs=[pl.BlockSpec(memory_space=pltpu.HBM)] * 16,
+        in_specs=[pl.BlockSpec(memory_space=pltpu.HBM)] * 13,
         out_specs=pl.BlockSpec(memory_space=pltpu.VMEM),
         scratch_shapes=[
             pltpu.VMEM((2, length, wide), bf16),
@@ -844,19 +852,16 @@
         name="whole_layer",
     )(
         tokens,
-        jnp.broadcast_to(mix_gain, (8, features)),
+        params,
         conv_b_weight,
         conv_c_weight,
         conv_v_weight,
-        jnp.concatenate([conv_taps, jnp.zeros((8 - conv_taps.shape[0], conv_taps.shape[1]), f32)], axis=0),
         query_weight,
         query_rope_weight,
         latent_weight,
         key_rope_weight.T,
-        jnp.broadcast_to(latent_gain, (8, n * lat_w)),
         key_up_weight,
         value_up_weight,
-        jnp.broadcast_to(head_gain, (8, head_gain.shape[0])),
         conv_out_weight,
         attn_out_weight,
     )

time: 110 us -> 109 us (level)
  local copies, waits for them, and re-layouts: 5.07 us -> 2.4 us
  other arithmetic: 0 us -> 1.36 us
    broadcast_in_dim x3 -> x0, local copies, waits for them, and re-layouts: 1.84 us -> none  [the longest x1 0.63 us: split_shards(): jnp.broadcast_to(mix_gain, (8, features))]
    concatenate x0 -> x2, other arithmetic: none -> 1.36 us  [the longest x1 0.7 us: split_shards(): gains = row(jnp.concatenate([latent_gain, head_gain]))]
    concatenate x1 -> x0, local copies, waits for them, and re-layouts: 1.31 us -> none  [split_shards(): jnp.concatenate([conv_taps, jnp.zeros((8 - conv_taps.shape[0], conv_taps....]
where the time goes in v3:
time: 109 us
  Pallas kernels  105 us (96%)
  local copies, waits for them, and re-layouts  2.4 us (2%)
  other arithmetic  1.36 us (1%)
    pallas_call x1, Pallas kernels, split_shards(): pl.pallas_call(functools.partial(layer_kernel, n, turns), out_shape=jax.S...  105 us
    unnamed x7, local copies, waits for them, and re-layouts  2.4 us

profile of v3, /device:TPU:0, one launch (start us, length us, event | category | flops | bytes accessed | tf_op | source)
XLA Modules:
  0.0 108.6 jit_solution(17179218458524518764)
XLA Ops:
  0.0 0.0 copy-start.2
  0.0 0.0 copy-start.1
  0.0 0.7 copy-done.2
  0.7 0.0 copy-start
  0.7 0.7 select_maximum_fusion.1
  1.4 0.0 copy-done.1
  1.4 0.0 copy-done
  1.4 0.7 select_maximum_fusion.params
  2.0 104.8 %whole_layer.1 = bf16[80,2048]{1,0:T(8,128)(2,1)} custom-call(bf16[1,160,1024]{2,1,0:T(8,128)(2,1)} %tok_in.1, f32[8,2048]{1,0:T(8,128)} %select_maximum_fusion.params, bf16[128,512]{1,0:T(8,128)(2,1)} %cb.1, bf16[128,512]{1,0:T(8,128)(2,1)} %cc.1, bf16[128,512]{1,0:T(8,128)(2,1)} %cv.1, bf16[128,1024]{1,0:T(8,128)(2,1)} %qw.1, bf16[128,512]{1,0:T(8,128)(2,1)} %qr.1, ...), custom_call_target="tpu_custom_call" | custom-call | tf_op jit(solution)/shard_map/whole_layer/pallas_call | solution.py:811
  106.9 1.7 %copy.18 = bf16[1,80,2048]{2,1,0:T(8,128)(2,1)} copy(bf16[1,80,2048]{2,1,0:T(8,128)(2,1)} %bitcast.4) | data formatting | bytes 655360
Async XLA Ops:
  0.0 0.7 copy-start.2
  0.0 1.4 %copy-start.1 = (f32[2048]{0:T(1024)S(1)}, f32[2048]{0:T(1024)}, u32[]{:S(2)}) copy-start(f32[2048]{0:T(1024)} %param.17) | copy-start | bytes 24580
  0.7 0.7 copy-start
